TPU v7x, 32 devices: a whole 2x2x4 slice. The times are simulated.
32 devices in a mesh: sp: 16 (over z, y, x), tp: 2 (over core).
Axes of the slice: x: 2, y: 2, z: 4, core: 2. Of those that a mesh axis runs over, the one named last changes fastest.
Arguments:
- tokens: bfloat16 [4096, 3072], P('sp', 'tp'), may hold values from -6 to 6
- norm_gain: float32 [3072], replicated, may hold values from 0.1 to 1.9
- outer_gate_w: bfloat16 [3072, 1536], P('sp', 'tp'), may hold values from -0.109375 to 0.109375
- inner_gate_w: bfloat16 [3072, 1536], P('sp', 'tp'), may hold values from -0.109375 to 0.109375
- signal_w: bfloat16 [3072, 1536], P('sp', 'tp'), may hold values from -0.109375 to 0.109375
- conv_taps: float32 [3, 1536], P(None, 'tp'), may hold values from -3.5 to 3.5
- query_w: bfloat16 [3072, 1536], P('sp', 'tp'), may hold values from -1.5 to 1.5
- key_w: bfloat16 [3072, 512], P('sp', 'tp'), may hold values from -1.5 to 1.5
- value_w: bfloat16 [3072, 512], P('sp', 'tp'), may hold values from -0.109375 to 0.109375
- sink_logits: float32 [24], P('tp'), may hold values from -1 to 5
- out_conv_w: bfloat16 [1536, 3072], P('tp', 'sp'), may hold values from -0.109375 to 0.109375
- out_attn_w: bfloat16 [1536, 3072], P('tp', 'sp'), may hold values from -0.109375 to 0.109375
Outputs:
- mixed: bfloat16 [4096, 3072], P(('sp', 'tp'))
All inputs are finite; a program needn't handle non-finite values.
Results may differ from a plain program's by a relative error of at most 0.02.
Values may be sent and summed in bfloat16 or wider, within the bound.
A program may use at most 64 MiB of HBM per device.

v0:
```python
import functools

import jax
import jax.numpy as jnp
from jax import lax
from jax.experimental import pallas as pl
from jax.experimental.pallas import tpu as pltpu
from jax.sharding import PartitionSpec as P

QHEADS = 24
KVHEADS = 8
HEAD = 64
TAPS = 3
WINDOW = 128
PLANE = 4
MESH = pl.DeviceIdType.MESH


def from_behind(value, axis, steps):
    count = lax.axis_size(axis)
    initial, last = (max(0, -steps), min(count, count - steps))
    return lax.ppermute(value, axis, [(source, source + steps) for source in range(initial, last)])


def add_products(pieces, normed):
    return tuple((jnp.dot(normed, piece, preferred_element_type=jnp.float32) for piece in pieces))


def convolve(gated, before, outer, conv_taps):
    extended = jnp.concatenate([before, gated], axis=0).astype(jnp.float32)
    length = gated.shape[0]
    conv = sum((conv_taps[k] * extended[k : k + length] for k in range(conv_taps.shape[0])))
    return (outer.astype(jnp.float32) * conv).astype(jnp.bfloat16)


def attention(queries, keys_ext, values_ext, sink_logits, offset):
    f32 = jnp.float32
    length = queries.shape[0]
    kv_local = keys_ext.shape[1] // HEAD
    group = QHEADS // KVHEADS
    heads_local = kv_local * group
    span = min(512, length)
    first = lax.axis_index("tp") * heads_local + 1
    slopes = jnp.exp2(
        -8.0 * (first + jnp.arange(heads_local, dtype=jnp.int32)).astype(f32) / QHEADS
    ).reshape(kv_local, group)
    sinks = sink_logits.reshape(kv_local, group)[:, :, None]

    def attend(block):
        start = block * span
        qblock = queries.reshape(span, kv_local, group, HEAD)
        kblock = keys_ext.reshape(span + WINDOW, kv_local, HEAD)
        vblock = values_ext.reshape(span + WINDOW, kv_local, HEAD)
        scores = jnp.einsum(
            "qhgd,shd->hgqs", qblock, kblock, preferred_element_type=f32
        ) * HEAD ** (-0.5)
        qpos = offset + start + jnp.arange(span, dtype=jnp.int32)
        kpos = offset + start - WINDOW + jnp.arange(span + WINDOW, dtype=jnp.int32)
        dist = qpos[:, None] - kpos[None, :]
        valid = (dist >= 0) & (dist < WINDOW) & (kpos >= 0)[None, :]
        scores = scores - slopes[:, :, None, None] * dist.astype(f32)
        scores = jnp.where(valid, scores, -1e30)
        top = jnp.maximum(jnp.max(scores, axis=-1), sinks)
        expo = jnp.exp(scores - top[..., None])
        total = jnp.sum(expo, axis=-1) + jnp.exp(sinks - top)
        probs = (expo / total[..., None]).astype(jnp.bfloat16)
        out = jnp.einsum("hgqs,shd->qhgd", probs, vblock, preferred_element_type=f32)
        return out.reshape(span, heads_local * HEAD)

    blocks = lax.map(attend, jnp.arange(length // span, dtype=jnp.int32))
    return blocks.reshape(length, heads_local * HEAD).astype(jnp.bfloat16)


def body(
    tokens,
    norm_gain,
    outer_gate_w,
    inner_gate_w,
    signal_w,
    conv_taps,
    query_w,
    key_w,
    value_w,
    sink_logits,
    out_conv_w,
    out_attn_w,
):
    f32 = jnp.float32
    bf16 = jnp.bfloat16
    whole = lax.all_gather(tokens, "tp", axis=1, tiled=True)
    x32 = whole.astype(f32)
    normed = (
        x32 * lax.rsqrt(jnp.mean(x32 * x32, axis=-1, keepdims=True) + 1e-06) * norm_gain
    ).astype(bf16)
    length = normed.shape[0]
    offset = lax.axis_index("sp") * length

    def fold_rows(pieces):
        return add_products(pieces, normed)

    conv_weights = (outer_gate_w, inner_gate_w, signal_w)
    conv_results = fold_rows(
        (
            lax.all_gather(conv_weights[0], "sp", axis=0, tiled=True),
            lax.all_gather(conv_weights[1], "sp", axis=0, tiled=True),
            lax.all_gather(conv_weights[2], "sp", axis=0, tiled=True),
        )
    )
    outer, inner, signal = tuple((result.astype(bf16) for result in conv_results))
    gated = (inner.astype(f32) * signal.astype(f32)).astype(bf16)
    before = from_behind(gated[length - TAPS + 1 :], "sp", 1)
    conv_out = convolve(gated, before, outer, conv_taps)
    attn_weights = (query_w, key_w, value_w)
    attn_results = fold_rows(
        (
            lax.all_gather(attn_weights[0], "sp", axis=0, tiled=True),
            lax.all_gather(attn_weights[1], "sp", axis=0, tiled=True),
            lax.all_gather(attn_weights[2], "sp", axis=0, tiled=True),
        )
    )
    queries, keys, values = tuple((result.astype(bf16) for result in attn_results))
    keys_before, values_before = from_behind(
        (keys[length - WINDOW :], values[length - WINDOW :]), "sp", 1
    )
    keys_ext = jnp.concatenate([keys_before, keys], axis=0)
    values_ext = jnp.concatenate([values_before, values], axis=0)
    attn_out = attention(queries, keys_ext, values_ext, sink_logits, offset)
    conv_whole, attn_whole = (
        lax.all_gather(out_conv_w, "sp", axis=1, tiled=True),
        lax.all_gather(out_attn_w, "sp", axis=1, tiled=True),
    )
    result = jnp.dot(conv_out, conv_whole, preferred_element_type=f32)
    mixed = lax.psum_scatter(
        (result + jnp.dot(attn_out, attn_whole, preferred_element_type=f32)).astype(jnp.bfloat16),
        "tp",
        scatter_dimension=0,
        tiled=True,
    ).astype(jnp.float32)
    return mixed.astype(bf16)


def start_to(src, dst, send_sem, recv_sem, target):
    copy = pltpu.make_async_remote_copy(
        src_ref=src,
        dst_ref=dst,
        send_sem=send_sem,
        recv_sem=recv_sem,
        device_id=target,
        device_id_type=MESH,
    )
    copy.start()
    return copy


def place(count):
    me, core = lax.axis_index("sp"), lax.axis_index("tp")
    return me, core, me // PLANE, lax.rem(me, PLANE), count // PLANE


def greet(me, core, layer, spot, layers):
    barrier = pltpu.get_barrier_semaphore()

    def signal(target):
        pl.semaphore_signal(barrier, inc=1, device_id=target, device_id_type=MESH)

    for k in range(1, PLANE):
        signal({"sp": layer * PLANE + lax.rem(spot + k, PLANE), "tp": core})
    signal({"sp": me, "tp": 1 - core})

    @pl.when(layer + 1 < layers)
    def _():
        signal({"sp": me + PLANE, "tp": core})

    @pl.when(layer > 0)
    def _():
        signal({"sp": me - PLANE, "tp": core})

    beside = jnp.where(layer + 1 < layers, 1, 0) + jnp.where(layer > 0, 1, 0)
    pl.semaphore_wait(barrier, PLANE + beside)


def gather_in_kernel(count, tok_ref, w_ref, gain_ref, out_ref, x_ref, wg_ref, nrm_ref, acc_ref, ws, wr, ts, tr, ds, dr, us, ur, vs, vr):
    me, core, layer, spot, layers = place(count)
    rows, half = tok_ref.shape
    partner = {"sp": me, "tp": 1 - core}
    above = {"sp": me + PLANE, "tp": core}
    below = {"sp": me - PLANE, "tp": core}
    greet(me, core, layer, spot, layers)

    def peer(k):
        return lax.rem(spot + k, PLANE)

    def source(k):
        return lax.rem(spot + PLANE - k, PLANE)

    def x_slot(p):
        return x_ref.at[core, pl.ds(pl.multiple_of(p * rows, rows), rows)]

    def z_copy(up, d, k, own):
        p = source(k)
        origin = layer - d if up else layer + d
        src = w_ref.at[spot] if own else wg_ref.at[origin, p]
        sems, semr = (us, ur) if up else (vs, vr)
        return pltpu.make_async_remote_copy(
            src_ref=src,
            dst_ref=wg_ref.at[origin, p],
            send_sem=sems.at[d, k],
            recv_sem=semr.at[d, k],
            device_id=above if up else below,
            device_id_type=MESH,
        )

    def z_arrive(up, d, k):
        p = source(k)
        origin = layer - d if up else layer + d
        sems, semr = (us, ur) if up else (vs, vr)
        pltpu.make_async_remote_copy(
            src_ref=w_ref.at[spot],
            dst_ref=wg_ref.at[origin, p],
            send_sem=sems.at[d - 1, k],
            recv_sem=semr.at[d - 1, k],
            device_id=above if up else below,
            device_id_type=MESH,
        ).wait_recv()

    def both(d, k, own, action):
        if d < layers - 1:
            @pl.when((layer + 1 < layers) & (layer >= d))
            def _():
                getattr(z_copy(True, d, k, own), action)()

            @pl.when((layer > 0) & (layer + d < layers))
            def _():
                getattr(z_copy(False, d, k, own), action)()

    both(0, 0, True, "start")
    w_copies = [
        start_to(w_ref.at[peer(k)], wg_ref.at[layer, spot], ws.at[k], wr.at[k], {"sp": layer * PLANE + peer(k), "tp": core})
        for k in range(1, PLANE)
    ]
    t_copies = [
        start_to(tok_ref, x_slot(spot), ts.at[k], tr.at[k], {"sp": layer * PLANE + peer(k), "tp": core})
        for k in range(1, PLANE)
    ]
    d_copies = [start_to(tok_ref, x_slot(spot), ds.at[0], dr.at[0], partner)]
    x_ref[core, pl.ds(pl.multiple_of(spot * rows, rows), rows), :] = tok_ref[...]
    wg_ref[layer, spot] = w_ref[spot]
    for k in range(1, PLANE):
        pltpu.make_async_remote_copy(
            src_ref=w_ref.at[spot], dst_ref=wg_ref.at[layer, source(k)], send_sem=ws.at[k], recv_sem=wr.at[k],
            device_id=partner, device_id_type=MESH,
        ).wait_recv()
        both(0, k, False, "start")

    def receive_layer(d):
        for k in range(PLANE):
            @pl.when(layer >= d)
            def _():
                z_arrive(True, d, k)

            @pl.when((layer >= d) & (layer + 1 < layers))
            def _():
                if d < layers - 1:
                    z_copy(True, d, k, False).start()

            @pl.when(layer + d < layers)
            def _():
                z_arrive(False, d, k)

            @pl.when((layer + d < layers) & (layer > 0))
            def _():
                if d < layers - 1:
                    z_copy(False, d, k, False).start()

    if layers > 1:
        receive_layer(1)
    for k in range(1, PLANE):
        p = source(k)
        pltpu.make_async_remote_copy(
            src_ref=tok_ref, dst_ref=x_slot(p), send_sem=ts.at[k], recv_sem=tr.at[k],
            device_id=partner, device_id_type=MESH,
        ).wait_recv()
        d_copies.append(start_to(x_slot(p), x_slot(p), ds.at[k], dr.at[k], partner))
    for k in range(PLANE):
        pltpu.make_async_remote_copy(
            src_ref=tok_ref,
            dst_ref=x_ref.at[1 - core, pl.ds(pl.multiple_of(source(k) * rows, rows), rows)],
            send_sem=ds.at[k], recv_sem=dr.at[k], device_id=partner, device_id_type=MESH,
        ).wait_recv()
    length = PLANE * rows
    span = 2 * half // layers
    strip, tall = 32, 256

    def normalise(i, carry):
        at = pl.ds(pl.multiple_of(i * strip, strip), strip)
        whole = jnp.concatenate([x_ref[0, at, :], x_ref[1, at, :]], axis=1).astype(jnp.float32)
        mean = jnp.sum(whole * whole, axis=1, keepdims=True) / (2 * half)
        scaled = (whole * lax.rsqrt(mean + 1e-06) * gain_ref[...]).astype(jnp.bfloat16)
        for j in range(layers):
            nrm_ref[j, at, :] = scaled[:, j * span : (j + 1) * span]
        return carry

    lax.fori_loop(0, length // strip, normalise, 0)

    def add_layer(origin, fresh):
        def step(i, carry):
            at = pl.ds(pl.multiple_of(i * tall, tall), tall)
            product = jnp.dot(
                nrm_ref[origin, at, :],
                wg_ref[origin].reshape(span, wg_ref.shape[3]),
                preferred_element_type=jnp.float32,
            )
            acc_ref[at, :] = product if fresh else acc_ref[at, :] + product
            return carry

        lax.fori_loop(0, length // tall, step, 0)

    def add_both(d):
        @pl.when(layer >= d)
        def _():
            add_layer(layer - d, False)

        @pl.when(layer + d < layers)
        def _():
            add_layer(layer + d, False)

    for d in range(2, layers - 1):
        receive_layer(d)
    add_layer(layer, True)
    for d in range(1, layers - 1):
        add_both(d)
    if layers > 2:
        receive_layer(layers - 1)
    if layers > 1:
        add_both(layers - 1)
    out_ref[...] = acc_ref[...].astype(out_ref.dtype)
    for copy in w_copies + t_copies + d_copies:
        copy.wait_send()
    for d in range(layers - 1):
        for k in range(PLANE):
            both(d, k, d == 0 and k == 0, "wait_send")


def gather_in(count, tokens, wblocks, gain):
    layers = count // PLANE
    rows, half = tokens.shape
    _, depth, cols = wblocks.shape
    dma = pltpu.SemaphoreType.DMA
    hops = max(layers - 1, 1)
    return pl.pallas_call(
        functools.partial(gather_in_kernel, count),
        out_shape=jax.ShapeDtypeStruct((PLANE * rows, cols), jnp.bfloat16),
        in_specs=[pl.BlockSpec(memory_space=pltpu.VMEM)] * 3,
        out_specs=pl.BlockSpec(memory_space=pltpu.VMEM),
        scratch_shapes=[
            pltpu.VMEM((2, PLANE * rows, half), tokens.dtype),
            pltpu.VMEM((layers, PLANE, depth, cols), wblocks.dtype),
            pltpu.VMEM((layers, PLANE * rows, 2 * half // layers), jnp.bfloat16),
            pltpu.VMEM((PLANE * rows, cols), jnp.float32),
        ]
        + [dma((PLANE,))] * 6
        + [dma((hops, PLANE))] * 4,
        compiler_params=pltpu.CompilerParams(
            collective_id=0, has_side_effects=True, vmem_limit_bytes=48 << 20
        ),
    )(tokens, wblocks, gain)


def gather_out_kernel(count, h_ref, o_ref, hg_ref, og_ref, held, lsem, ts, tr, ds, dr, us, ur, vs, vr, es, er, fs):
    me, core, layer, spot, layers = place(count)
    width = h_ref.shape[1]
    cols, depth = o_ref.shape
    half = cols // 2
    partner = {"sp": me, "tp": 1 - core}
    above = {"sp": me + PLANE, "tp": core}
    below = {"sp": me - PLANE, "tp": core}
    greet(me, core, layer, spot, layers)

    def peer(k):
        return lax.rem(spot + k, PLANE)

    def source(k):
        return lax.rem(spot + PLANE - k, PLANE)

    def h_slot(c, p):
        return hg_ref.at[:, pl.ds(pl.multiple_of((c * PLANE + p) * width, width), width)]

    def z_copy(up, d, sem_d):
        origin = layer - d if up else layer + d
        sems, semr = (us, ur) if up else (vs, vr)
        return pltpu.make_async_remote_copy(
            src_ref=o_ref if d == 0 else held.at[origin],
            dst_ref=held.at[origin],
            send_sem=sems.at[sem_d],
            recv_sem=semr.at[sem_d],
            device_id=above if up else below,
            device_id_type=MESH,
        )

    def og_slot(origin, c):
        return og_ref.at[pl.ds(pl.multiple_of(origin * half, half), half), pl.ds(pl.multiple_of(c * depth, depth), depth)]

    def part(ref, c):
        return ref.at[pl.ds(pl.multiple_of(c * half, half), half)]

    def pieces(ref, origin, slot):
        swap = pltpu.make_async_remote_copy(
            src_ref=part(ref, 1 - core), dst_ref=og_slot(origin, core), send_sem=es.at[slot], recv_sem=er.at[slot],
            device_id=partner, device_id_type=MESH,
        )
        keep = pltpu.make_async_copy(part(ref, core), og_slot(origin, core), fs.at[slot])
        return swap, keep

    def on_block(up, d, action):
        origin = layer - d if up else layer + d
        if d == 0:
            swap, keep = pieces(o_ref, layer, 0)
        else:
            swap, keep = pieces(held.at[origin], origin, d if up else layers - 1 + d)
        if action == "start":
            swap.start()
            keep.start()
        else:
            swap.wait_send()
            keep.wait()
            pltpu.make_async_remote_copy(
                src_ref=part(o_ref, core), dst_ref=og_slot(origin, 1 - core), send_sem=es.at[0],
                recv_sem=er.at[0 if d == 0 else (d if up else layers - 1 + d)],
                device_id=partner, device_id_type=MESH,
            ).wait_recv()

    def send(d, action):
        if d < layers - 1:
            @pl.when((layer + 1 < layers) & (layer >= d))
            def _():
                getattr(z_copy(True, d, d), action)()

            @pl.when((layer > 0) & (layer + d < layers))
            def _():
                getattr(z_copy(False, d, d), action)()

    send(0, "start")
    t_copies = [
        start_to(h_ref, h_slot(core, spot), ts.at[k], tr.at[k], {"sp": layer * PLANE + peer(k), "tp": core})
        for k in range(1, PLANE)
    ]
    d_copies = [start_to(h_ref, h_slot(core, spot), ds.at[0], dr.at[0], partner)]
    local = pltpu.make_async_copy(h_ref, h_slot(core, spot), lsem.at[0])
    local.start()
    on_block(True, 0, "start")

    def receive_layer(d):
        @pl.when(layer >= d)
        def _():
            z_copy(True, d, d - 1).wait_recv()
            on_block(True, d, "start")

        @pl.when(layer + d < layers)
        def _():
            z_copy(False, d, d - 1).wait_recv()
            on_block(False, d, "start")

        send(d, "start")

    for d in range(1, max(layers - 1, 1)):
        receive_layer(d)
    for k in range(1, PLANE):
        p = source(k)
        pltpu.make_async_remote_copy(
            src_ref=h_ref, dst_ref=h_slot(core, p), send_sem=ts.at[k], recv_sem=tr.at[k],
            device_id=partner, device_id_type=MESH,
        ).wait_recv()
        d_copies.append(start_to(h_slot(core, p), h_slot(core, p), ds.at[k], dr.at[k], partner))
    if layers > 1:
        receive_layer(layers - 1)
    for copy in t_copies:
        copy.wait_send()
    for k, copy in enumerate(d_copies):
        copy.wait_send()
        pltpu.make_async_remote_copy(
            src_ref=h_ref, dst_ref=h_slot(1 - core, source(k)), send_sem=ds.at[k], recv_sem=dr.at[k],
            device_id=partner, device_id_type=MESH,
        ).wait_recv()
    on_block(True, 0, "wait")
    for d in range(layers):
        send(d, "wait_send")
    for d in range(1, layers):
        @pl.when(layer >= d)
        def _():
            on_block(True, d, "wait")

        @pl.when(layer + d < layers)
        def _():
            on_block(False, d, "wait")
    local.wait()


def gather_out(count, hidden, out_t):
    layers = count // PLANE
    rows, width = hidden.shape
    cols, depth = out_t.shape
    dma = pltpu.SemaphoreType.DMA
    hops = max(layers - 1, 1)
    return pl.pallas_call(
        functools.partial(gather_out_kernel, count),
        out_shape=(
            jax.ShapeDtypeStruct((rows, 2 * PLANE * width), hidden.dtype),
            jax.ShapeDtypeStruct((layers * cols // 2, 2 * depth), out_t.dtype),
        ),
        in_specs=[pl.BlockSpec(memory_space=pltpu.VMEM)] * 2,
        out_specs=[pl.BlockSpec(memory_space=pl.ANY)] * 2,
        scratch_shapes=[pltpu.VMEM((layers, cols, depth), out_t.dtype), dma((1,))]
        + [dma((PLANE,))] * 4
        + [dma((hops,))] * 4
        + [dma((2 * layers,))] * 3,
        compiler_params=pltpu.CompilerParams(collective_id=1, has_side_effects=True),
    )(hidden, out_t)


def exchange_kernel(h_ref, o_ref, out_ref, y_ref, ss, rs):
    me, core = lax.axis_index("sp"), lax.axis_index("tp")
    spot = lax.rem(me, PLANE)
    first = me - spot
    mine = spot * 2 + core
    group = 2 * PLANE

    def target(k):
        other = lax.rem(mine + k, group)
        return other, {"sp": first + other // 2, "tp": lax.rem(other, 2)}

    barrier = pltpu.get_barrier_semaphore()
    for k in range(1, group):
        pl.semaphore_signal(barrier, inc=1, device_id=target(k)[1], device_id_type=MESH)
    pl.semaphore_wait(barrier, group - 1)
    rows = out_ref.shape[1]

    def product(other):
        at = pl.ds(pl.multiple_of(other * rows, rows), rows)
        return lax.dot_general(
            h_ref[at, :], o_ref[...], (((1,), (1,)), ((), ())), preferred_element_type=jnp.float32
        ).astype(out_ref.dtype)

    copies = []

    def send(k):
        copies.append(start_to(y_ref.at[k], out_ref.at[mine], ss.at[k], rs.at[k], target(k)[1]))

    for k in range(1, group):
        y_ref[k] = product(target(k)[0])
        if k > 1:
            send(k - 1)
    out_ref[mine] = product(mine)
    send(group - 1)
    for k in range(1, group):
        copies[k - 1].wait_send()
        pltpu.make_async_remote_copy(
            src_ref=y_ref.at[0], dst_ref=out_ref.at[lax.rem(mine + group - k, group)], send_sem=ss.at[k],
            recv_sem=rs.at[k], device_id=target(k)[1], device_id_type=MESH,
        ).wait_recv()


def exchange(hidden, out_t):
    dma = pltpu.SemaphoreType.DMA
    blocks = (2 * PLANE, hidden.shape[0] // (2 * PLANE), out_t.shape[0])
    return pl.pallas_call(
        exchange_kernel,
        out_shape=jax.ShapeDtypeStruct(blocks, hidden.dtype),
        in_specs=[pl.BlockSpec(memory_space=pltpu.VMEM)] * 2,
        out_specs=pl.BlockSpec(memory_space=pltpu.VMEM),
        scratch_shapes=[pltpu.VMEM(blocks, hidden.dtype), dma((2 * PLANE,)), dma((2 * PLANE,))],
        compiler_params=pltpu.CompilerParams(
            collective_id=2, has_side_effects=True, vmem_limit_bytes=40 << 20
        ),
    )(hidden, out_t)


def pack_kernel(*refs):
    *weights, out_ref = refs
    for p in range(PLANE):
        pieces = []
        for ref in weights:
            width = ref.shape[1] // PLANE
            pieces.append(ref[:, p * width : (p + 1) * width])
        out_ref[p] = jnp.concatenate(pieces, axis=1)


def pack(weights):
    depth = weights[0].shape[0]
    cols = sum(w.shape[1] for w in weights) // PLANE
    return pl.pallas_call(
        pack_kernel,
        out_shape=jax.ShapeDtypeStruct((PLANE, depth, cols), weights[0].dtype),
        in_specs=[pl.BlockSpec(memory_space=pltpu.VMEM)] * len(weights),
        out_specs=pl.BlockSpec(memory_space=pltpu.VMEM),
    )(*weights)


def mixer_kernel(chans, wide, slopes_ref, sinks_ref, offset_ref, proj_ref, before_ref, kv_before_ref, taps_ref, out_ref, ext, gext):
    f32, bf16 = jnp.float32, jnp.bfloat16
    length = proj_ref.shape[0]
    group = wide // HEAD
    front = 8
    ext[0:WINDOW] = kv_before_ref[...]
    ext[WINDOW:] = proj_ref[:, 3 * chans + wide :]
    gext[0:front] = jnp.concatenate(
        [jnp.zeros((front - TAPS + 1, chans), f32), before_ref[...].astype(f32)], axis=0
    )
    row = lax.broadcasted_iota(jnp.int32, (WINDOW, 2 * WINDOW), 0)
    col = lax.broadcasted_iota(jnp.int32, (WINDOW, 2 * WINDOW), 1)
    dist = WINDOW + row - col
    near = (dist >= 0) & (dist < WINDOW)
    far = dist.astype(f32)

    def block(i, carry):
        start = pl.multiple_of(i * WINDOW, WINDOW)
        rows = pl.ds(start, WINDOW)
        chunk = proj_ref[rows, :]
        inner = chunk[:, chans : 2 * chans].astype(f32)
        signal = chunk[:, 2 * chans : 3 * chans].astype(f32)
        gext[pl.ds(pl.multiple_of(start + front, 8), WINDOW), :] = (inner * signal).astype(bf16).astype(f32)
        window = gext[pl.ds(start, WINDOW + front), :]
        conv = sum(
            taps_ref[k : k + 1, :] * window[front - TAPS + 1 + k : front - TAPS + 1 + k + WINDOW]
            for k in range(TAPS)
        )
        pieces = [(chunk[:, :chans].astype(f32) * conv).astype(bf16)]
        kv = ext[pl.ds(start, 2 * WINDOW), :]
        keys, values = kv[:, :HEAD], kv[:, HEAD:]
        valid = near & (offset_ref[0] + start - WINDOW + col >= 0)
        for g in range(group):
            first = 3 * chans + g * HEAD
            scores = lax.dot_general(
                chunk[:, first : first + HEAD], keys, (((1,), (1,)), ((), ())), preferred_element_type=f32
            ) * HEAD ** (-0.5)
            scores = jnp.where(valid, scores - slopes_ref[g] * far, -1e30)
            sink = sinks_ref[g]
            top = jnp.maximum(jnp.max(scores, axis=1, keepdims=True), sink)
            expo = jnp.exp(scores - top)
            total = jnp.sum(expo, axis=1, keepdims=True) + jnp.exp(sink - top)
            probs = (expo / total).astype(bf16)
            pieces.append(jnp.dot(probs, values, preferred_element_type=f32).astype(bf16))
        out_ref[rows, :] = jnp.concatenate(pieces, axis=1)
        return carry

    lax.fori_loop(0, length // WINDOW, block, 0)


def mixer(proj, before, kv_before, taps, slopes, sinks, offset, wide):
    length = proj.shape[0]
    chans = taps.shape[1]
    smem = pl.BlockSpec(memory_space=pltpu.SMEM)
    vmem = pl.BlockSpec(memory_space=pltpu.VMEM)
    return pl.pallas_call(
        functools.partial(mixer_kernel, chans, wide),
        out_shape=jax.ShapeDtypeStruct((length, chans + wide), jnp.bfloat16),
        in_specs=[smem] * 3 + [vmem] * 4,
        out_specs=vmem,
        scratch_shapes=[
            pltpu.VMEM((WINDOW + length, 2 * HEAD), jnp.bfloat16),
            pltpu.VMEM((8 + length, chans), jnp.float32),
        ],
    )(slopes, sinks, jnp.reshape(offset, (1,)), proj, before, kv_before, taps)


def plane_body(
    tokens,
    norm_gain,
    outer_gate_w,
    inner_gate_w,
    signal_w,
    conv_taps,
    query_w,
    key_w,
    value_w,
    sink_logits,
    out_conv_w,
    out_attn_w,
):
    f32 = jnp.float32
    bf16 = jnp.bfloat16
    count = lax.axis_size("sp")
    layers = count // PLANE
    me, core = lax.axis_index("sp"), lax.axis_index("tp")
    layer, spot = me // PLANE, lax.rem(me, PLANE)
    chans = outer_gate_w.shape[1] // PLANE
    wide = query_w.shape[1] // PLANE
    group = QHEADS // KVHEADS

    wblocks = pack((outer_gate_w, inner_gate_w, signal_w, query_w, key_w, value_w))
    proj = gather_in(count, tokens, wblocks, norm_gain.reshape(1, -1))
    length = proj.shape[0]
    last = proj[length - TAPS + 1 :, chans : 3 * chans].astype(f32)
    before = from_behind((last[:, :chans] * last[:, chans:]).astype(bf16), "sp", PLANE)
    kv_before = from_behind(proj[length - WINDOW :, 3 * chans + wide :], "sp", PLANE)
    taps = lax.dynamic_slice_in_dim(conv_taps, spot * chans, chans, 1)
    head = (core * PLANE + spot) * group + 1 + jnp.arange(group, dtype=jnp.int32)
    slopes = jnp.exp2(-8.0 * head.astype(f32) / QHEADS)
    sinks = lax.dynamic_slice_in_dim(sink_logits, spot * group, group, 0)
    hidden = mixer(proj, before, kv_before, taps, slopes, sinks, layer * length, wide)
    cols = out_conv_w.shape[1]
    out_t = jnp.concatenate(
        [out_conv_w.reshape(PLANE, chans, cols), out_attn_w.reshape(PLANE, wide, cols)], axis=1
    ).reshape(-1, cols).T
    hidden_all, out_all = gather_out(count, hidden, out_t)
    swapped = exchange(hidden_all, out_all)
    rows = length // (2 * PLANE)
    swapped = swapped.reshape(PLANE, 2, rows, layers, cols // 2).transpose(2, 3, 0, 1, 4)
    return swapped.reshape(rows, -1)


def solution(mesh):
    kv_local = KVHEADS // mesh.shape["tp"]
    fits = mesh.shape["tp"] == 2 and kv_local == PLANE and mesh.shape["sp"] % PLANE == 0
    chosen = plane_body if fits else body
    in_specs = (
        P("sp", "tp"),
        P(),
        P("sp", "tp"),
        P("sp", "tp"),
        P("sp", "tp"),
        P(None, "tp"),
        P("sp", "tp"),
        P("sp", "tp"),
        P("sp", "tp"),
        P("tp"),
        P("tp", "sp"),
        P("tp", "sp"),
    )
    out_specs = P(("sp", "tp"), None)
    return jax.shard_map(chosen, mesh=mesh, in_specs=in_specs, out_specs=out_specs, check_vma=False)
```

profile of v0, /device:TPU:0, one launch (start us, length us, event | category | flops | bytes accessed | tf_op | source)
XLA Modules:
  0.0 192.5 jit_solution(9542996347511746867)
XLA Ops:
  0.0 0.0 copy-start
  0.0 0.0 copy-start.6
  0.0 0.0 copy-start.5
  0.0 2.8 %shard_map.118.w_ref = bf16[4,192,896]{2,1,0:T(8,128)(2,1)} custom-call(bf16[192,768]{1,0:T(8,128)(2,1)} %refs_0_.1, bf16[192,768]{1,0:T(8,128)(2,1)} %refs_1_.1, bf16[192,768]{1,0:T(8,128)(2,1)} %refs_2_.1, bf16[192,768]{1,0:T(8,128)(2,1)} %refs_3_.1, bf16[192,256]{1,0:T(8,128)(2,1)} %refs_4_.1, bf16[192,256]{1,0:T(8,128)(2,1)} %refs_5_.1), custom_call_target="tpu_custom_call" | custom-call | tf_op jit(solution)/shard_map/pallas_call | solution.py:590
  2.8 0.0 copy-done.6
  2.8 0.0 copy-done.5
  2.8 0.0 copy-start.3
  2.8 1.3 copy-done.3
  4.1 0.0 copy-start.7
  4.1 0.0 copy-start.8
  4.1 99.0 %shard_map.119.proj_ref = bf16[1024,896]{1,0:T(8,128)(2,1)S(1)} custom-call(bf16[256,1536]{1,0:T(8,128)(2,1)S(1)} %copy-done.5, bf16[4,192,896]{2,1,0:T(8,128)(2,1)S(1)} %copy-done.3, f32[1,3072]{1,0:T(1,128)S(1)} %bitcast.16), custom_call_target="tpu_custom_call" | custom-call | tf_op jit(solution)/shard_map/pallas_call | solution.py:350
  103.2 0.0 copy-start.1
  103.2 0.1 slice_convert_fusion
  103.3 0.9 fusion
  104.1 1.3 collective-permute-start
  105.4 0.6 slice.15
  106.0 1.3 collective-permute-start.1
  107.3 0.0 copy-done.7
  107.4 0.0 copy-start.11
  107.4 0.4 reshape.23
  107.7 0.0 copy-done.8
  107.7 0.4 reshape.24
  108.1 0.0 copy-done
  108.1 0.7 constant_dynamic-slice_fusion.taps_ref
  108.8 0.5 pad_maximum_fusion
  109.3 0.5 multiply_exponential_fusion.slopes_ref
  109.8 1.0 copy.17
  110.8 0.0 copy-done.1
  110.8 0.0 copy-done.11
  110.8 0.6 dynamic_slice.6.sinks_ref
  111.4 0.0 collective-permute-done.before_ref
  111.4 0.0 copy-start.10
  111.4 0.0 collective-permute-done.1.kv_before_ref
  111.4 0.0 copy-start.9
  111.4 0.6 copy-done.10
  112.0 0.0 copy-done.9
  112.0 10.4 %shard_map.120.h_ref = bf16[1024,384]{1,0:T(8,128)(2,1)} custom-call(f32[3]{0:T(128)} %multiply_exponential_fusion.slopes_ref, f32[3]{0:T(128)} %dynamic_slice.6.sinks_ref, s32[1]{0:T(128)} %bitcast.offset_ref, bf16[1024,896]{1,0:T(8,128)(2,1)} %copy-done.1, bf16[2,192]{1,0:T(2,128)(2,1)} %copy-done.10, bf16[128,128]{1,0:T(8,128)(2,1)} %copy-done.9, ...), custom_call_target="tpu_custom_call" | custom-call | tf_op jit(solution)/shard_map/pallas_call | solution.py:653
  122.4 47.2 %shard_map.121 = (bf16[1024,3072]{1,0:T(8,128)(2,1)}, bf16[384,3072]{1,0:T(8,128)(2,1)}) custom-call(bf16[1024,384]{1,0:T(8,128)(2,1)} %shard_map.120.h_ref, bf16[192,1536]{1,0:T(8,128)(2,1)} %bitcast.19), custom_call_target="tpu_custom_call" | custom-call | tf_op jit(solution)/shard_map/pallas_call | solution.py:504
  169.7 0.0 copy-start.2
  169.7 2.8 %copy-done.2 = bf16[1024,3072]{1,0:T(8,128)(2,1)S(1)} copy-done((bf16[1024,3072]{1,0:T(8,128)(2,1)S(1)}, bf16[1024,3072]{1,0:T(8,128)(2,1)}, u32[]{:S(2)}) %copy-start.2) | copy-done | bytes 6291480
  172.5 0.0 copy-start.4
  172.5 1.7 copy-done.4
  174.1 16.7 %shard_map.122 = bf16[8,128,384]{2,1,0:T(8,128)(2,1)S(1)} custom-call(bf16[1024,3072]{1,0:T(8,128)(2,1)S(1)} %copy-done.2, bf16[384,3072]{1,0:T(8,128)(2,1)S(1)} %copy-done.4), custom_call_target="tpu_custom_call" | custom-call | tf_op jit(solution)/shard_map/pallas_call | solution.py:565
  190.9 0.4 copy.14
  191.3 0.1 copy.15
  191.3 1.2 copy.16
Async XLA Ops:
  0.0 108.1 %copy-start = (f32[3,768]{1,0:T(4,128)S(1)}, f32[3,768]{1,0:T(4,128)}, u32[]{:S(2)}) copy-start(f32[3,768]{1,0:T(4,128)} %param.17) | copy-start | bytes 27652
  0.0 2.8 %copy-start.6 = (f32[3072]{0:T(1024)S(1)}, f32[3072]{0:T(1024)}, u32[]{:S(2)}) copy-start(f32[3072]{0:T(1024)} %param.13) | copy-start | bytes 36868
  0.0 2.8 %copy-start.5 = (bf16[256,1536]{1,0:T(8,128)(2,1)S(1)}, bf16[256,1536]{1,0:T(8,128)(2,1)}, u32[]{:S(2)}) copy-start(bf16[256,1536]{1,0:T(8,128)(2,1)} %tok_ref.1) | copy-start | bytes 2359300
  2.8 1.3 copy-start.3
  4.1 103.2 %copy-start.7 = (bf16[768,192]{0,1:T(8,128)(2,1)S(1)}, bf16[768,192]{0,1:T(8,128)(2,1)}, u32[]{:S(2)}) copy-start(bf16[768,192]{0,1:T(8,128)(2,1)} %param.22) | copy-start | bytes 884740
  4.1 103.6 %copy-start.8 = (bf16[768,192]{0,1:T(8,128)(2,1)S(1)}, bf16[768,192]{0,1:T(8,128)(2,1)}, u32[]{:S(2)}) copy-start(bf16[768,192]{0,1:T(8,128)(2,1)} %param.23) | copy-start | bytes 884740
  103.2 7.6 %copy-start.1 = (bf16[1024,896]{1,0:T(8,128)(2,1)}, bf16[1024,896]{1,0:T(8,128)(2,1)S(1)}, u32[]{:S(2)}) copy-start(bf16[1024,896]{1,0:T(8,128)(2,1)S(1)} %shard_map.119.proj_ref) | copy-start | bytes 5505028
  104.1 7.3 %collective-permute-start = (bf16[2,192]{1,0:T(2,128)(2,1)}, bf16[2,192]{1,0:T(2,128)(2,1)S(1)}, u32[]{:S(2)}, u32[]{:S(2)}) collective-permute-start(bf16[2,192]{1,0:T(2,128)(2,1)} %fusion), channel_id=1, source_target_pairs={{0,8},{2,10},{4,12},{6,14},{8,16},{10,18},{12,20},{14,22},{16,24},... | collective-permute-start | bytes 2312 | tf_op jit(solution)/shard_map/ppermute | solution.py:22
  106.0 5.4 %collective-permute-start.1 = (bf16[128,128]{1,0:T(8,128)(2,1)}, bf16[128,128]{1,0:T(8,128)(2,1)S(1)}, u32[]{:S(2)}, u32[]{:S(2)}) collective-permute-start(bf16[128,128]{1,0:T(8,128)(2,1)} %slice.15), channel_id=1, source_target_pairs={{0,8},{2,10},{4,12},{6,14},{8,16},{10,18},{12,20},{14,22},{16,24},... | collective-permute-start | bytes 98312 | tf_op jit(solution)/shard_map/ppermute | solution.py:22
  107.4 3.4 %copy-start.11 = (f32[12]{0:T(128)S(1)}, f32[12]{0:T(128)}, u32[]{:S(2)}) copy-start(f32[12]{0:T(128)} %param.21) | copy-start | bytes 148
  111.4 0.6 copy-start.10
  111.4 0.6 copy-start.9
  169.7 2.8 %copy-start.2 = (bf16[1024,3072]{1,0:T(8,128)(2,1)S(1)}, bf16[1024,3072]{1,0:T(8,128)(2,1)}, u32[]{:S(2)}) copy-start(bf16[1024,3072]{1,0:T(8,128)(2,1)} %get-tuple-element.7.h_ref) | copy-start | bytes 18874372
  172.5 1.7 copy-start.4
where the time goes:
time: 193 us
  Pallas kernels  176 us (91%)
  local copies, waits for them, and re-layouts  11.6 us (6%)
  starting transfers between devices  2.56 us (1%)
    pallas_call x1, Pallas kernels, gather_in(): pl.pallas_call(functools.partial(gather_in_kernel, count), out_shape=jax....  99 us
    pallas_call x1, Pallas kernels, gather_out(): pl.pallas_call(functools.partial(gather_out_kernel, count), out_shape=(ja...  47.2 us
    pallas_call x1, Pallas kernels, exchange(): pl.pallas_call(exchange_kernel, out_shape=jax.ShapeDtypeStruct(blocks, hi...  16.7 us
    pallas_call x1, Pallas kernels, mixer(): pl.pallas_call(functools.partial(mixer_kernel, chans, wide), out_shape=ja...  10.4 us
    unnamed x25, local copies, waits for them, and re-layouts  7.39 us
  transfers between devices with their start and end apart: 2, of which 0 were waited for; matrix products, arithmetic and copies ran while one was open for 2% of the time, Pallas kernels for 0%

commit v1 on v0

v1 whole, which is shorter than its diff:
```python
import functools

import jax
import jax.numpy as jnp
from jax import lax
from jax.experimental import pallas as pl
from jax.experimental.pallas import tpu as pltpu
from jax.sharding import PartitionSpec as P

QHEADS = 24
KVHEADS = 8
HEAD = 64
TAPS = 3
WINDOW = 128
PLANE = 4
MESH = pl.DeviceIdType.MESH


def from_behind(value, axis, steps):
    count = lax.axis_size(axis)
    initial, last = (max(0, -steps), min(count, count - steps))
    return lax.ppermute(value, axis, [(source, source + steps) for source in range(initial, last)])


def add_products(pieces, normed):
    return tuple((jnp.dot(normed, piece, preferred_element_type=jnp.float32) for piece in pieces))


def convolve(gated, before, outer, conv_taps):
    extended = jnp.concatenate([before, gated], axis=0).astype(jnp.float32)
    length = gated.shape[0]
    conv = sum((conv_taps[k] * extended[k : k + length] for k in range(conv_taps.shape[0])))
    return (outer.astype(jnp.float32) * conv).astype(jnp.bfloat16)


def attention(queries, keys_ext, values_ext, sink_logits, offset):
    f32 = jnp.float32
    length = queries.shape[0]
    kv_local = keys_ext.shape[1] // HEAD
    group = QHEADS // KVHEADS
    heads_local = kv_local * group
    span = min(512, length)
    first = lax.axis_index("tp") * heads_local + 1
    slopes = jnp.exp2(
        -8.0 * (first + jnp.arange(heads_local, dtype=jnp.int32)).astype(f32) / QHEADS
    ).reshape(kv_local, group)
    sinks = sink_logits.reshape(kv_local, group)[:, :, None]

    def attend(block):
        start = block * span
        qblock = queries.reshape(span, kv_local, group, HEAD)
        kblock = keys_ext.reshape(span + WINDOW, kv_local, HEAD)
        vblock = values_ext.reshape(span + WINDOW, kv_local, HEAD)
        scores = jnp.einsum(
            "qhgd,shd->hgqs", qblock, kblock, preferred_element_type=f32
        ) * HEAD ** (-0.5)
        qpos = offset + start + jnp.arange(span, dtype=jnp.int32)
        kpos = offset + start - WINDOW + jnp.arange(span + WINDOW, dtype=jnp.int32)
        dist = qpos[:, None] - kpos[None, :]
        valid = (dist >= 0) & (dist < WINDOW) & (kpos >= 0)[None, :]
        scores = scores - slopes[:, :, None, None] * dist.astype(f32)
        scores = jnp.where(valid, scores, -1e30)
        top = jnp.maximum(jnp.max(scores, axis=-1), sinks)
        expo = jnp.exp(scores - top[..., None])
        total = jnp.sum(expo, axis=-1) + jnp.exp(sinks - top)
        probs = (expo / total[..., None]).astype(jnp.bfloat16)
        out = jnp.einsum("hgqs,shd->qhgd", probs, vblock, preferred_element_type=f32)
        return out.reshape(span, heads_local * HEAD)

    blocks = lax.map(attend, jnp.arange(length // span, dtype=jnp.int32))
    return blocks.reshape(length, heads_local * HEAD).astype(jnp.bfloat16)


def body(
    tokens,
    norm_gain,
    outer_gate_w,
    inner_gate_w,
    signal_w,
    conv_taps,
    query_w,
    key_w,
    value_w,
    sink_logits,
    out_conv_w,
    out_attn_w,
):
    f32 = jnp.float32
    bf16 = jnp.bfloat16
    whole = lax.all_gather(tokens, "tp", axis=1, tiled=True)
    x32 = whole.astype(f32)
    normed = (
        x32 * lax.rsqrt(jnp.mean(x32 * x32, axis=-1, keepdims=True) + 1e-06) * norm_gain
    ).astype(bf16)
    length = normed.shape[0]
    offset = lax.axis_index("sp") * length

    def fold_rows(pieces):
        return add_products(pieces, normed)

    conv_weights = (outer_gate_w, inner_gate_w, signal_w)
    conv_results = fold_rows(
        (
            lax.all_gather(conv_weights[0], "sp", axis=0, tiled=True),
            lax.all_gather(conv_weights[1], "sp", axis=0, tiled=True),
            lax.all_gather(conv_weights[2], "sp", axis=0, tiled=True),
        )
    )
    outer, inner, signal = tuple((result.astype(bf16) for result in conv_results))
    gated = (inner.astype(f32) * signal.astype(f32)).astype(bf16)
    before = from_behind(gated[length - TAPS + 1 :], "sp", 1)
    conv_out = convolve(gated, before, outer, conv_taps)
    attn_weights = (query_w, key_w, value_w)
    attn_results = fold_rows(
        (
            lax.all_gather(attn_weights[0], "sp", axis=0, tiled=True),
            lax.all_gather(attn_weights[1], "sp", axis=0, tiled=True),
            lax.all_gather(attn_weights[2], "sp", axis=0, tiled=True),
        )
    )
    queries, keys, values = tuple((result.astype(bf16) for result in attn_results))
    keys_before, values_before = from_behind(
        (keys[length - WINDOW :], values[length - WINDOW :]), "sp", 1
    )
    keys_ext = jnp.concatenate([keys_before, keys], axis=0)
    values_ext = jnp.concatenate([values_before, values], axis=0)
    attn_out = attention(queries, keys_ext, values_ext, sink_logits, offset)
    conv_whole, attn_whole = (
        lax.all_gather(out_conv_w, "sp", axis=1, tiled=True),
        lax.all_gather(out_attn_w, "sp", axis=1, tiled=True),
    )
    result = jnp.dot(conv_out, conv_whole, preferred_element_type=f32)
    mixed = lax.psum_scatter(
        (result + jnp.dot(attn_out, attn_whole, preferred_element_type=f32)).astype(jnp.bfloat16),
        "tp",
        scatter_dimension=0,
        tiled=True,
    ).astype(jnp.float32)
    return mixed.astype(bf16)

class Stream:
    def __init__(self, at, src, buf, sems, split):
        self.at, self.src, self.buf, self.split = at, src, buf, split
        self.zs, self.zr, self.ys, self.yr, self.xs, self.xr = sems
        self.rows = src.shape[1] // split

    def part(self, s):
        return pl.ds(s * self.rows, self.rows)

    def slot(self, t, origin, y, x, s):
        return self.buf.at[t, origin, y, x, self.part(s)]

    def origin(self, up, d):
        return self.at.z - d if up else self.at.z + d

    def column(self, r):
        return self.at.x if r == 0 else 1 - self.at.x

    def z_copy(self, up, d, r, t, s, send_d):
        at = self.at
        dst = self.slot(t, self.origin(up, d), at.y, self.column(r), s)
        src = self.src.at[2 * t + at.x, self.part(s)] if d == 0 and r == 0 else dst
        i = ((((0 if up else 1) * (at.layers - 1) + send_d) * 2 + r) * 2 + t) * self.split + s
        return remote(src, dst, self.zs.at[i], self.zr.at[i], at.above if up else at.below)

    def z_send(self, up, d, r, t, s, action="start"):
        z, layers = self.at.z, self.at.layers
        if d >= layers - 1:
            return
        if up:
            go = (z >= d) & (z + (1 if t else 2) < layers)
        else:
            go = (z + d < layers) & (z >= (2 if t else 1))

        @pl.when(go)
        def _():
            getattr(self.z_copy(up, d, r, t, s, d), action)()

    def y_copy(self, up, d, r, s, y):
        at = self.at
        dst = self.slot(at.zl, self.origin(up, d), y, self.column(r), s)
        src = self.src.at[2 * at.zl + at.x, self.part(s)] if d == 0 and r == 0 else dst
        m = d if up or d == 0 else at.layers - 1 + d
        i = (m * 2 + r) * self.split + s
        return remote(src, dst, self.ys.at[i], self.yr.at[i], at.ypeer)

    def x_copy(self, t, s, receive=False):
        at = self.at
        src = self.src.at[2 * t + 1 - at.x, self.part(s)]
        dst = self.slot(t, at.z, at.y, 1 - at.x if receive else at.x, s)
        i = t * self.split + s
        return remote(src, dst, self.xs.at[i], self.xr.at[i], at.xpeer)

    def start_z(self):
        for s in range(self.split):
            for t in range(2):
                self.z_send(True, 0, 0, 1 - t, s)
                self.z_send(False, 0, 0, t, s)

    def start_x(self):
        for s in range(self.split):
            for t in range(2):
                self.x_copy(t, s).start()

    def start_y(self):
        for s in range(self.split):
            self.y_copy(True, 0, 0, s, self.at.y).start()

    def on_x(self):
        for s in range(self.split):
            for t in range(2):
                self.x_copy(t, s, True).wait_recv()
                self.z_send(True, 0, 1, t, s)
                self.z_send(False, 0, 1, t, s)

                @pl.when(self.at.zl == t)
                def _():
                    self.y_copy(True, 0, 1, s, self.at.y).start()

    def on_z(self, d, r):
        z, layers, zl = self.at.z, self.at.layers, self.at.zl

        def arrive(up, t, s):
            if up:
                here = (z >= d) if t else (z >= d) & (z + 1 < layers)
            else:
                here = (z + d < layers) & (z >= 1) if t else (z + d < layers)

            @pl.when(here)
            def _():
                self.z_copy(up, d, r, t, s, d - 1).wait_recv()
                self.z_send(up, d, r, t, s)

                @pl.when(zl == t)
                def _():
                    self.y_copy(up, d, r, s, self.at.y).start()

        for s in range(self.split):
            for t in range(2):
                arrive(True, 1 - t, s)
                arrive(False, t, s)

    def on_y(self, d, action="wait_recv"):
        z, layers, y = self.at.z, self.at.layers, self.at.y
        side = 1 - y if action == "wait_recv" else y

        def each(up):
            for r in range(2):
                for s in range(self.split):
                    getattr(self.y_copy(up, d, r, s, side), action)()

        if d == 0:
            each(True)
            return

        @pl.when(z >= d)
        def _():
            each(True)

        @pl.when(z + d < layers)
        def _():
            each(False)

    def finish(self):
        for s in range(self.split):
            for t in range(2):
                self.x_copy(t, s).wait_send()
        for d in range(self.at.layers):
            self.on_y(d, "wait_send")
            for r in range(2):
                for t in range(2):
                    for s in range(self.split):
                        self.z_send(True, d, r, t, s, "wait_send")
                        self.z_send(False, d, r, t, s, "wait_send")


class Place:
    def __init__(self, count):
        me, core = lax.axis_index("sp"), lax.axis_index("tp")
        self.me, self.core, self.layers = me, core, count // PLANE
        self.z, self.y, self.x = me // PLANE, lax.rem(me // 2, 2), lax.rem(me, 2)
        self.zl, self.zh = lax.rem(self.z, 2), self.z // 2
        self.spot = 2 * self.zl + self.x

        def device(sp, tp=core):
            return {"sp": sp, "tp": tp}

        self.partner = device(me, 1 - core)
        self.xpeer = device(me + 1 - 2 * self.x)
        self.ypeer = device(me + 2 - 4 * self.y)
        self.zpeer = device(me + PLANE * (1 - 2 * self.zl))
        self.above, self.below = device(me + PLANE), device(me - PLANE)
        self.after, self.prior = device(me + PLANE + 2), device(me - PLANE - 2)
        self.has_after = (self.y == 1) & (self.zh + 1 < self.layers // 2)
        self.has_prior = (self.y == 0) & (self.zh > 0)

    def greet(self):
        barrier = pltpu.get_barrier_semaphore()

        def signal(target):
            pl.semaphore_signal(barrier, inc=1, device_id=target, device_id_type=MESH)

        for target in (self.partner, self.xpeer, self.ypeer):
            signal(target)
        number = 3
        for go, target in (
            (self.z + 1 < self.layers, self.above),
            (self.z > 0, self.below),
            (self.has_after, self.after),
            (self.has_prior, self.prior),
        ):
            pl.when(go)(functools.partial(signal, target))
            number = number + jnp.where(go, 1, 0)
        pl.semaphore_wait(barrier, number)


def remote(src, dst, send_sem, recv_sem, target):
    return pltpu.make_async_remote_copy(
        src_ref=src, dst_ref=dst, send_sem=send_sem, recv_sem=recv_sem, device_id=target, device_id_type=MESH
    )


def layer_kernel(
    count, chans, wide, split, slopes_ref, sinks_ref, tok_ref, w_ref, o_ref, gain_ref, taps_ref, out_ref,
    x_ref, nrm_ref, wbuf, obuf, acc_ref, ext, gext, hid, dsend, drecv, own, s1, r1, s2, r2,
    wzs, wzr, wys, wyr, wxs, wxr, ozs, ozr, oys, oyr, oxs, oxr, ts, tr, hs, hr, ds, dr, fs, fr, gs, gr,
):
    f32, bf16 = jnp.float32, jnp.bfloat16
    at = Place(count)
    core, layers, x, y, z, zl, zh, spot = at.core, at.layers, at.x, at.y, at.z, at.zl, at.zh, at.spot
    rows, half = tok_ref.shape
    length = 2 * rows
    group = wide // HEAD
    front = 8
    ins = Stream(at, w_ref, wbuf, (wzs, wzr, wys, wyr, wxs, wxr), split)
    outs = Stream(at, o_ref, obuf, (ozs, ozr, oys, oyr, oxs, oxr), 1)
    at.greet()

    def block(p, side=None):
        return x_ref.at[core if side is None else side, pl.ds(pl.multiple_of(p * rows, rows), rows)]

    p_own, p_x, p_z, p_far = spot, 2 * zl + 1 - x, 2 * (1 - zl) + x, 2 * (1 - zl) + 1 - x
    ins.start_z()
    ins.start_x()
    ins.start_y()
    tok_x = remote(tok_ref, block(p_own), ts.at[0], tr.at[0], at.xpeer)
    tok_z = remote(tok_ref, block(p_own), ts.at[1], tr.at[1], at.zpeer)
    tok_far = remote(block(p_z), block(p_z), ts.at[2], tr.at[2], at.xpeer)
    swaps = [
        remote(tok_ref if k == 0 else block(p), block(p), ts.at[3 + k], tr.at[3 + k], at.partner)
        for k, p in enumerate((p_own, p_x, p_z, p_far))
    ]
    tok_x.start()
    tok_z.start()
    swaps[0].start()
    wbuf[zl, z, y, x] = w_ref[2 * zl + x]
    x_ref[core, pl.ds(pl.multiple_of(p_own * rows, rows), rows), :] = tok_ref[...]
    span = 2 * half // layers
    strip = 32

    def normalise(k, p):
        remote(tok_ref, block(p, 1 - core), ts.at[3 + k], tr.at[3 + k], at.partner).wait_recv()

        def step(i, carry):
            at_rows = pl.ds(pl.multiple_of(p * rows + i * strip, strip), strip)
            whole = jnp.concatenate([x_ref[0, at_rows, :], x_ref[1, at_rows, :]], axis=1).astype(f32)
            mean = jnp.sum(whole * whole, axis=1, keepdims=True) / (2 * half)
            scaled = (whole * lax.rsqrt(mean + 1e-06) * gain_ref[...]).astype(bf16)
            for j in range(layers):
                nrm_ref[j, at_rows, :] = scaled[:, j * span : (j + 1) * span]
            return carry

        lax.fori_loop(0, rows // strip, step, 0)

    def add_layer(origin, fresh):
        def step(i, carry):
            at_rows = pl.ds(pl.multiple_of(i * rows, rows), rows)
            product = jnp.dot(
                nrm_ref[origin, at_rows, :],
                wbuf[zl, origin].reshape(span, wbuf.shape[5]),
                preferred_element_type=f32,
            )
            acc_ref[at_rows, :] = product if fresh else acc_ref[at_rows, :] + product
            return carry

        lax.fori_loop(0, PLANE, step, 0)

    def add_both(d):
        ins.on_y(d)

        @pl.when(z >= d)
        def _():
            add_layer(z - d, False)

        @pl.when(z + d < layers)
        def _():
            add_layer(z + d, False)

    ins.on_x()
    ins.on_z(1, 0)
    remote(tok_ref, block(p_z), ts.at[1], tr.at[1], at.zpeer).wait_recv()
    tok_far.start()
    swaps[2].start()
    outs.start_x()
    remote(tok_ref, block(p_x), ts.at[0], tr.at[0], at.xpeer).wait_recv()
    swaps[1].start()
    ins.on_z(1, 1)
    normalise(0, p_own)
    normalise(2, p_z)
    if layers > 2:
        ins.on_z(2, 0)
    normalise(1, p_x)
    remote(tok_ref, block(p_far), ts.at[2], tr.at[2], at.xpeer).wait_recv()
    swaps[3].start()
    if layers > 2:
        ins.on_z(2, 1)
    normalise(3, p_far)
    outs.start_z()
    ins.on_y(0)
    add_layer(z, True)
    for d in range(3, layers):
        ins.on_z(d, 0)
        ins.on_z(d, 1)
    add_both(1)
    outs.start_y()
    outs.on_x()
    obuf[zl, z, y, x] = o_ref[2 * zl + x]
    for d in range(2, layers):
        add_both(d)
    outs.on_z(1, 0)

    def spread(i, carry):
        run, start = i // 4, pl.multiple_of(lax.rem(i, 4) * WINDOW, WINDOW)
        chunk = acc_ref[pl.ds(pl.multiple_of(i * WINDOW, WINDOW), WINDOW), :].astype(bf16)
        ext[run, pl.ds(start + WINDOW, WINDOW), :] = chunk[:, 3 * chans + wide :]
        product = chunk[:, chans : 2 * chans].astype(f32) * chunk[:, 2 * chans : 3 * chans].astype(f32)
        gext[run, pl.ds(start + front, WINDOW), :] = product.astype(bf16).astype(f32)
        return carry

    lax.fori_loop(0, 2 * length // WINDOW, spread, 0)

    def tails(run, after, target, action):
        kv = remote(
            ext.at[run, pl.ds(length, WINDOW)], ext.at[after, pl.ds(0, WINDOW)],
            hs.at[2 * run], hr.at[2 * after], target,
        )
        gated = remote(
            gext.at[run, pl.ds(length, front)], gext.at[after, pl.ds(0, front)],
            hs.at[2 * run + 1], hr.at[2 * after + 1], target,
        )
        for copy in (kv, gated):
            getattr(copy, action)()

    def all_tails(action):
        @pl.when(y == 0)
        def _():
            for run in range(2):
                tails(run, run, at.ypeer, action)

        @pl.when(y == 1)
        def _():
            tails(0, 1, at.ypeer, action)

        @pl.when(at.has_after)
        def _():
            tails(1, 0, at.after, action)

    all_tails("start")
    first_run = (y == 0) & (zh == 0)

    @pl.when(first_run)
    def _():
        ext[0, 0:WINDOW, :] = jnp.zeros((WINDOW, 2 * HEAD), bf16)
        gext[0, 0:front, :] = jnp.zeros((front, chans), f32)

    taps = sum(jnp.where(spot == c, taps_ref[:, c * chans : (c + 1) * chans], 0.0) for c in range(PLANE))
    row = lax.broadcasted_iota(jnp.int32, (WINDOW, 2 * WINDOW), 0)
    col = lax.broadcasted_iota(jnp.int32, (WINDOW, 2 * WINDOW), 1)
    dist = WINDOW + row - col
    near = (dist >= 0) & (dist < WINDOW)
    far = dist.astype(f32)

    def mix(run, blk):
        start = pl.multiple_of(blk * WINDOW, WINDOW)
        chunk = acc_ref[pl.ds(pl.multiple_of(run * length + start, WINDOW), WINDOW), :].astype(bf16)
        window = gext[run, pl.ds(start, WINDOW + front), :]
        conv = sum(
            taps[k : k + 1, :] * window[front - TAPS + 1 + k : front - TAPS + 1 + k + WINDOW]
            for k in range(TAPS)
        )
        pieces = [(chunk[:, :chans].astype(f32) * conv).astype(bf16)]
        kv = ext[run, pl.ds(start, 2 * WINDOW), :]
        keys, values = kv[:, :HEAD], kv[:, HEAD:]
        offset = ((2 * zh + run) * 2 + y) * length
        valid = near & (offset + start - WINDOW + col >= 0)
        for g in range(group):
            first = 3 * chans + g * HEAD
            scores = lax.dot_general(
                chunk[:, first : first + HEAD], keys, (((1,), (1,)), ((), ())), preferred_element_type=f32
            ) * HEAD ** (-0.5)
            scores = jnp.where(valid, scores - slopes_ref[(core * PLANE + spot) * group + g] * far, -1e30)
            sink = sinks_ref[spot * group + g]
            top = jnp.maximum(jnp.max(scores, axis=1, keepdims=True), sink)
            expo = jnp.exp(scores - top)
            total = jnp.sum(expo, axis=1, keepdims=True) + jnp.exp(sink - top)
            probs = (expo / total).astype(bf16)
            pieces.append(jnp.dot(probs, values, preferred_element_type=f32).astype(bf16))
        place = pl.ds(pl.multiple_of((2 * run + blk // 2) * WINDOW, WINDOW), WINDOW)
        hid[lax.rem(blk, 2), place, :] = jnp.concatenate(pieces, axis=1)

    def inner_block(i, carry):
        mix(i // 3, 1 + lax.rem(i, 3))
        return carry

    def first_block(i, carry):
        mix(i, 0)
        return carry

    lax.fori_loop(0, 3, inner_block, 0)
    outs.on_z(1, 1)
    if layers > 2:
        outs.on_z(2, 0)
    lax.fori_loop(3, 6, inner_block, 0)
    if layers > 2:
        outs.on_z(2, 1)

    def tails_in(after, target):
        for k, (ref, size) in enumerate(((ext, WINDOW), (gext, front))):
            remote(
                ref.at[after, pl.ds(length, size)], ref.at[after, pl.ds(0, size)],
                hs.at[2 * after + k], hr.at[2 * after + k], target,
            ).wait_recv()

    @pl.when(y == 1)
    def _():
        tails_in(0, at.ypeer)

    @pl.when(at.has_prior)
    def _():
        tails_in(0, at.prior)

    tails_in(1, at.ypeer)
    lax.fori_loop(0, 2, first_block, 0)
    for d in range(3, layers):
        outs.on_z(d, 0)
        outs.on_z(d, 1)

    lower = z < layers // 2
    cols = obuf.shape[2] * obuf.shape[3] * obuf.shape[4]

    def chunk_at(i):
        return jnp.where(lower, i, layers - 1 - i)

    def product(side, i):
        return lax.dot_general(
            hid[side], obuf[zl, chunk_at(i)].reshape(cols, hid.shape[2]),
            (((1,), (1,)), ((), ())), preferred_element_type=f32,
        )

    def slab(p):
        return pl.ds(pl.multiple_of(p * WINDOW, WINDOW), WINDOW)

    def swap(i):
        return remote(dsend.at[i], drecv.at[i], ds.at[i], dr.at[i], at.partner)

    def first_hop(i, j):
        if i % 2 == 0:
            target, p = at.xpeer, (2 * (1 - zl) if j == 0 else 2 * zl) + 1 - x
        else:
            target, p = at.zpeer, 2 * (1 - zl) + ((1 - x) if j == 0 else x)
        return remote(s1.at[i, slab(p)], r1.at[i, j], fs.at[2 * i + j], fr.at[2 * i + j], target)

    def second_hop(i):
        return remote(s2.at[i], r2.at[i], gs.at[i], gr.at[i], at.zpeer if i % 2 == 0 else at.xpeer)

    def begin(i):
        dsend[i] = product(1 - core, i).astype(bf16)
        own[i % 2] = product(core, i)
        swap(i).start()

    def fold(i):
        swap(i).wait_recv()
        s1[i] = (own[i % 2] + drecv[i].astype(f32)).astype(bf16)
        first_hop(i, 0).start()
        first_hop(i, 1).start()

    def relay(i):
        first_hop(i, 0).wait_recv()
        p = p_z if i % 2 == 0 else p_x
        s2[i] = (s1[i, slab(p), :].astype(f32) + r1[i, 0].astype(f32)).astype(bf16)
        second_hop(i).start()

    def collect(i):
        first_hop(i, 1).wait_recv()
        second_hop(i).wait_recv()
        total = s1[i, slab(p_own), :].astype(f32) + r1[i, 1].astype(f32) + r2[i].astype(f32)
        out_ref[:, pl.ds(pl.multiple_of(chunk_at(i) * cols, cols), cols)] = total.astype(out_ref.dtype)

    ready = -1
    for i in range(layers):
        need = max(i, layers // 2 - 1 - i)
        while ready < need:
            ready += 1
            outs.on_y(ready)
        begin(i)
        if i > 0:
            fold(i - 1)
    fold(layers - 1)
    for i in range(layers):
        relay(i)
    for i in range(layers):
        collect(i)

    ins.finish()
    outs.finish()
    all_tails("wait_send")
    for copy in [tok_x, tok_z, tok_far] + swaps:
        copy.wait_send()
    for i in range(layers):
        swap(i).wait_send()
        first_hop(i, 0).wait_send()
        first_hop(i, 1).wait_send()
        second_hop(i).wait_send()


def whole_layer(count, tokens, wblocks, oblocks, gain, taps, slopes, sinks, wide):
    layers = count // PLANE
    rows, half = tokens.shape
    _, depth, width = wblocks.shape
    _, cols, inner = oblocks.shape
    chans = taps.shape[1] // PLANE
    bf16, f32 = jnp.bfloat16, jnp.float32
    dma = pltpu.SemaphoreType.DMA
    split = 2
    length = 2 * rows
    slab = 4 * cols

    def sems(parts):
        hops = 2 * (layers - 1) * 4 * parts
        return [dma((hops,))] * 2 + [dma(((2 * layers - 1) * 2 * parts,))] * 2 + [dma((2 * parts,))] * 2

    smem = pl.BlockSpec(memory_space=pltpu.SMEM)
    vmem = pl.BlockSpec(memory_space=pltpu.VMEM)
    return pl.pallas_call(
        functools.partial(layer_kernel, count, chans, wide, split),
        out_shape=jax.ShapeDtypeStruct((rows // 2, 2 * half), bf16),
        in_specs=[smem] * 2 + [vmem] * 5,
        out_specs=vmem,
        scratch_shapes=[
            pltpu.VMEM((2, PLANE * rows, half), bf16),
            pltpu.VMEM((layers, PLANE * rows, 2 * half // layers), bf16),
            pltpu.VMEM((2, layers, 2, 2, depth, width), bf16),
            pltpu.VMEM((2, layers, 2, 2, cols, inner), bf16),
            pltpu.VMEM((PLANE * rows, width), f32),
            pltpu.VMEM((2, WINDOW + length, 2 * HEAD), bf16),
            pltpu.VMEM((2, 8 + length, chans), f32),
            pltpu.VMEM((2, PLANE * WINDOW, inner), bf16),
            pltpu.VMEM((layers, PLANE * WINDOW, slab), bf16),
            pltpu.VMEM((layers, PLANE * WINDOW, slab), bf16),
            pltpu.VMEM((2, PLANE * WINDOW, slab), f32),
            pltpu.VMEM((layers, PLANE * WINDOW, slab), bf16),
            pltpu.VMEM((layers, 2, WINDOW, slab), bf16),
            pltpu.VMEM((layers, WINDOW, slab), bf16),
            pltpu.VMEM((layers, WINDOW, slab), bf16),
        ]
        + sems(split)
        + sems(1)
        + [dma((7,))] * 2
        + [dma((4,))] * 2
        + [dma((layers,))] * 2
        + [dma((2 * layers,))] * 2
        + [dma((layers,))] * 2,
        compiler_params=pltpu.CompilerParams(
            collective_id=0, has_side_effects=True, vmem_limit_bytes=60 << 20
        ),
    )(slopes, sinks, tokens, wblocks, oblocks, gain, taps)


def pack_kernel(*refs):
    *weights, out_ref = refs
    for p in range(PLANE):
        pieces = []
        for ref in weights:
            width = ref.shape[1] // PLANE
            pieces.append(ref[:, p * width : (p + 1) * width])
        out_ref[p] = jnp.concatenate(pieces, axis=1)


def pack(weights):
    depth = weights[0].shape[0]
    cols = sum(w.shape[1] for w in weights) // PLANE
    return pl.pallas_call(
        pack_kernel,
        out_shape=jax.ShapeDtypeStruct((PLANE, depth, cols), weights[0].dtype),
        in_specs=[pl.BlockSpec(memory_space=pltpu.VMEM)] * len(weights),
        out_specs=pl.BlockSpec(memory_space=pltpu.VMEM),
    )(*weights)


def plane_body(
    tokens,
    norm_gain,
    outer_gate_w,
    inner_gate_w,
    signal_w,
    conv_taps,
    query_w,
    key_w,
    value_w,
    sink_logits,
    out_conv_w,
    out_attn_w,
):
    if tokens.shape[0] != 2 * WINDOW:
        return body(
            tokens, norm_gain, outer_gate_w, inner_gate_w, signal_w, conv_taps,
            query_w, key_w, value_w, sink_logits, out_conv_w, out_attn_w,
        )
    count = lax.axis_size("sp")
    chans = outer_gate_w.shape[1] // PLANE
    wide = query_w.shape[1] // PLANE
    wblocks = pack((outer_gate_w, inner_gate_w, signal_w, query_w, key_w, value_w))
    cols = out_conv_w.shape[1]
    oblocks = jnp.concatenate(
        [out_conv_w.reshape(PLANE, chans, cols), out_attn_w.reshape(PLANE, wide, cols)], axis=1
    ).transpose(0, 2, 1)
    slopes = jnp.array([2.0 ** (-8.0 * h / QHEADS) for h in range(1, QHEADS + 1)], jnp.float32)
    return whole_layer(
        count, tokens, wblocks, oblocks, norm_gain.reshape(1, -1), conv_taps, slopes, sink_logits, wide
    )


def solution(mesh):
    kv_local = KVHEADS // mesh.shape["tp"]
    fits = mesh.shape["tp"] == 2 and kv_local == PLANE and mesh.shape["sp"] % (2 * PLANE) == 0
    chosen = plane_body if fits else body
    in_specs = (
        P("sp", "tp"),
        P(),
        P("sp", "tp"),
        P("sp", "tp"),
        P("sp", "tp"),
        P(None, "tp"),
        P("sp", "tp"),
        P("sp", "tp"),
        P("sp", "tp"),
        P("tp"),
        P("tp", "sp"),
        P("tp", "sp"),
    )
    out_specs = P(("sp", "tp"), None)
    return jax.shard_map(chosen, mesh=mesh, in_specs=in_specs, out_specs=out_specs, check_vma=False)
```

time: 193 us -> 142 us (0.74)
  Pallas kernels: 176 us -> 137 us
  local copies, waits for them, and re-layouts: 11.6 us -> 3.89 us
  starting transfers between devices: 2.56 us -> 0 us
    pallas_call x4 -> x1, Pallas kernels: 173 us -> 134 us  [whole_layer(): pl.pallas_call(functools.partial(layer_kernel, count, chans, wide, split)...]
    unnamed x25 -> x3, local copies, waits for them, and re-layouts: 7.39 us -> 2.07 us
    ppermute x2 -> x0, starting transfers between devices: 2.56 us -> none  [from_behind(): lax.ppermute(value, axis, [(source, source + steps) for source in range(i...]
  transfers between devices with their start and end apart: 2 -> 0, of which waited for: 0 -> 0; matrix products, arithmetic and copies ran while one was open for 2% -> 0% of each run, Pallas kernels for 0% -> 0%
where the time goes in v1:
time: 142 us
  Pallas kernels  137 us (96%)
  local copies, waits for them, and re-layouts  3.89 us (3%)
    pallas_call x1, Pallas kernels, whole_layer(): pl.pallas_call(functools.partial(layer_kernel, count, chans, wide, split)...  134 us

profile of v1, /device:TPU:0, one launch (start us, length us, event | category | flops | bytes accessed | tf_op | source)
XLA Modules:
  0.0 142.0 jit_solution(18382212070483648197)
XLA Ops:
  0.0 0.0 copy-start
  0.0 1.4 reshape.9
  1.4 0.0 copy-done
  1.4 0.4 reshape.10
  1.9 1.0 maximum_bitcast_fusion.o_ref
  2.9 2.7 %shard_map.127.w_ref = bf16[4,192,896]{2,1,0:T(8,128)(2,1)} custom-call(bf16[192,768]{1,0:T(8,128)(2,1)} %refs_0_.1, bf16[192,768]{1,0:T(8,128)(2,1)} %refs_1_.1, bf16[192,768]{1,0:T(8,128)(2,1)} %refs_2_.1, bf16[192,768]{1,0:T(8,128)(2,1)} %refs_3_.1, bf16[192,256]{1,0:T(8,128)(2,1)} %refs_4_.1, bf16[192,256]{1,0:T(8,128)(2,1)} %refs_5_.1), custom_call_target="tpu_custom_call" | custom-call | tf_op jit(solution)/shard_map/pallas_call | solution.py:692
  5.6 134.3 %shard_map.128 = bf16[128,3072]{1,0:T(8,128)(2,1)} custom-call(f32[24]{0:T(128)} %constant.2.clone.slopes_ref, f32[12]{0:T(128)} %sinks_ref.1, bf16[256,1536]{1,0:T(8,128)(2,1)} %tok_ref.1, bf16[4,192,896]{2,1,0:T(8,128)(2,1)} %shard_map.127.w_ref, bf16[4,192,384]{2,1,0:T(8,128)(2,1)} %maximum_bitcast_fusion.o_ref, f32[1,3072]{1,0:T(1,128)} %bitcast.7, ...), custom_call_target="tpu_custom_call" | custom-call | tf_op jit(solution)/shard_map/pallas_call | solution.py:644
  139.9 2.1 %copy.17 = bf16[128,3072]{1,0:T(8,128)(2,1)} copy(bf16[128,3072]{1,0:T(8,128)(2,1)} %shard_map.128) | data formatting | bytes 1572864
  (2 shorter events, 0.1 us)
Async XLA Ops:
  0.0 1.4 %copy-start = (bf16[768,192]{0,1:T(8,128)(2,1)S(1)}, bf16[768,192]{0,1:T(8,128)(2,1)}, u32[]{:S(2)}) copy-start(bf16[768,192]{0,1:T(8,128)(2,1)} %param.24) | copy-start | bytes 884740

commit v2 on v1

--- a/solution.py
+++ b/solution.py
@@ -13,6 +13,9 @@
 TAPS = 3
 WINDOW = 128
 PLANE = 4
+LAYERS = 4
+PAIR, APART, BOTH = 1, 2, 3
+FAR, NEAR = (0,), (1,)
 MESH = pl.DeviceIdType.MESH
 
 
@@ -163,7 +166,7 @@
         i = ((((0 if up else 1) * (at.layers - 1) + send_d) * 2 + r) * 2 + t) * self.split + s
         return remote(src, dst, self.zs.at[i], self.zr.at[i], at.above if up else at.below)
 
-    def z_send(self, up, d, r, t, s, action="start"):
+    def z_send(self, up, d, r, t, s, action="start", only=True):
         z, layers = self.at.z, self.at.layers
         if d >= layers - 1:
             return
@@ -172,7 +175,7 @@
         else:
             go = (z + d < layers) & (z >= (2 if t else 1))
 
-        @pl.when(go)
+        @pl.when(go & only)
         def _():
             getattr(self.z_copy(up, d, r, t, s, d), action)()
 
@@ -191,42 +194,39 @@
         i = t * self.split + s
         return remote(src, dst, self.xs.at[i], self.xr.at[i], at.xpeer)
 
-    def start_z(self):
-        for s in range(self.split):
-            for t in range(2):
-                self.z_send(True, 0, 0, 1 - t, s)
-                self.z_send(False, 0, 0, t, s)
+    def send_z(self, r, s, which=FAR + NEAR, only=True):
+        for k in which:
+            self.z_send(True, 0, r, 1 - k, s, only=only)
+            self.z_send(False, 0, r, k, s, only=only)
 
     def start_x(self):
         for s in range(self.split):
             for t in range(2):
                 self.x_copy(t, s).start()
 
-    def start_y(self):
-        for s in range(self.split):
-            self.y_copy(True, 0, 0, s, self.at.y).start()
-
-    def on_x(self):
-        for s in range(self.split):
-            for t in range(2):
-                self.x_copy(t, s, True).wait_recv()
-                self.z_send(True, 0, 1, t, s)
-                self.z_send(False, 0, 1, t, s)
-
-                @pl.when(self.at.zl == t)
-                def _():
-                    self.y_copy(True, 0, 1, s, self.at.y).start()
-
-    def on_z(self, d, r):
+    def wait_x(self, s):
+        for t in range(2):
+            self.x_copy(t, s, True).wait_recv()
+
+    def send_y(self, r, s, only=True):
+        @pl.when(only)
+        def _():
+            self.y_copy(True, 0, r, s, self.at.y).start()
+
+    def on_z(self, d, r, s, which=FAR + NEAR, sides=BOTH, only=True):
         z, layers, zl = self.at.z, self.at.layers, self.at.zl
 
-        def arrive(up, t, s):
+        def arrive(up, t):
             if up:
                 here = (z >= d) if t else (z >= d) & (z + 1 < layers)
             else:
                 here = (z + d < layers) & (z >= 1) if t else (z + d < layers)
-
-            @pl.when(here)
+            if sides == PAIR:
+                here = here & (zl == (1 if up else 0))
+            elif sides == APART:
+                here = here & (zl == (0 if up else 1))
+
+            @pl.when(here & only)
             def _():
                 self.z_copy(up, d, r, t, s, d - 1).wait_recv()
                 self.z_send(up, d, r, t, s)
@@ -235,13 +235,12 @@
                 def _():
                     self.y_copy(up, d, r, s, self.at.y).start()
 
-        for s in range(self.split):
-            for t in range(2):
-                arrive(True, 1 - t, s)
-                arrive(False, t, s)
-
-    def on_y(self, d, action="wait_recv"):
-        z, layers, y = self.at.z, self.at.layers, self.at.y
+        for k in which:
+            arrive(True, 1 - k)
+            arrive(False, k)
+
+    def on_y(self, d, action="wait_recv", sides=BOTH):
+        z, layers, y, zl = self.at.z, self.at.layers, self.at.y, self.at.zl
         side = 1 - y if action == "wait_recv" else y
 
         def each(up):
@@ -253,11 +252,16 @@
             each(True)
             return
 
-        @pl.when(z >= d)
+        from_below, from_above = z >= d, z + d < layers
+        if sides != BOTH:
+            near = 1 if sides == PAIR else 0
+            from_below, from_above = from_below & (zl == near), from_above & (zl == 1 - near)
+
+        @pl.when(from_below)
         def _():
             each(True)
 
-        @pl.when(z + d < layers)
+        @pl.when(from_above)
         def _():
             each(False)
 
@@ -274,6 +278,15 @@
                         self.z_send(False, d, r, t, s, "wait_send")
 
 
+def join(weights, out_ref):
+    for p in range(PLANE):
+        pieces = []
+        for ref in weights:
+            width = ref.shape[1] // PLANE
+            pieces.append(ref[:, p * width : (p + 1) * width])
+        out_ref[p] = jnp.concatenate(pieces, axis=1)
+
+
 class Place:
     def __init__(self, count):
         me, core = lax.axis_index("sp"), lax.axis_index("tp")
@@ -311,7 +324,7 @@
         ):
             pl.when(go)(functools.partial(signal, target))
             number = number + jnp.where(go, 1, 0)
-        pl.semaphore_wait(barrier, number)
+        return lambda: pl.semaphore_wait(barrier, number)
 
 
 def remote(src, dst, send_sem, recv_sem, target):
@@ -320,46 +333,91 @@
     )
 
 
+def layer_entry(
+    count, chans, wide, split, slopes_ref, sinks_ref, tok_hbm, *refs,
+):
+    raw_hbm, (gain_hbm, taps_hbm, out_ref), refs = refs[:8], refs[8:11], refs[11:]
+    raw, refs = refs[:8], refs[8:]
+    layer_kernel(count, chans, wide, split, slopes_ref, sinks_ref, tok_hbm, raw_hbm, gain_hbm, taps_hbm, out_ref, raw, *refs)
+
+
 def layer_kernel(
-    count, chans, wide, split, slopes_ref, sinks_ref, tok_ref, w_ref, o_ref, gain_ref, taps_ref, out_ref,
-    x_ref, nrm_ref, wbuf, obuf, acc_ref, ext, gext, hid, dsend, drecv, own, s1, r1, s2, r2,
+    count, chans, wide, split, slopes_ref, sinks_ref, tok_hbm, raw_hbm, gain_hbm, taps_hbm, out_ref, raw,
+    gain_ref, taps_ref, w_ref, o_ref, ls, x_ref, nrm_ref, wbuf, obuf, acc_ref, ext, gext, hid, dsend, drecv, own, s1, r1, s2, r2,
     wzs, wzr, wys, wyr, wxs, wxr, ozs, ozr, oys, oyr, oxs, oxr, ts, tr, hs, hr, ds, dr, fs, fr, gs, gr,
 ):
     f32, bf16 = jnp.float32, jnp.bfloat16
     at = Place(count)
     core, layers, x, y, z, zl, zh, spot = at.core, at.layers, at.x, at.y, at.z, at.zl, at.zh, at.spot
-    rows, half = tok_ref.shape
+    rows, half = tok_hbm.shape
     length = 2 * rows
     group = wide // HEAD
     front = 8
     ins = Stream(at, w_ref, wbuf, (wzs, wzr, wys, wyr, wxs, wxr), split)
     outs = Stream(at, o_ref, obuf, (ozs, ozr, oys, oyr, oxs, oxr), 1)
-    at.greet()
+    arrived = at.greet()
 
     def block(p, side=None):
         return x_ref.at[core if side is None else side, pl.ds(pl.multiple_of(p * rows, rows), rows)]
 
     p_own, p_x, p_z, p_far = spot, 2 * zl + 1 - x, 2 * (1 - zl) + x, 2 * (1 - zl) + 1 - x
-    ins.start_z()
+    loads = [
+        pltpu.make_async_copy(src, dst, ls.at[k])
+        for k, (src, dst) in enumerate(
+            list(zip(raw_hbm[:6], raw[:6]))
+            + [(tok_hbm, block(p_own))]
+            + list(zip(raw_hbm[6:], raw[6:]))
+            + [(gain_hbm, gain_ref), (taps_hbm, taps_ref)]
+        )
+    ]
+    for load in loads:
+        load.start()
+    for load in loads[:6]:
+        load.wait()
+    join(raw[:6], w_ref)
+    loads[6].wait()
+    arrived()
+    at_end = (z == 0) | (z == layers - 1)
+    inside = jnp.logical_not(at_end)
+    ins.send_z(0, 0, FAR)
     ins.start_x()
-    ins.start_y()
-    tok_x = remote(tok_ref, block(p_own), ts.at[0], tr.at[0], at.xpeer)
-    tok_z = remote(tok_ref, block(p_own), ts.at[1], tr.at[1], at.zpeer)
-    tok_far = remote(block(p_z), block(p_z), ts.at[2], tr.at[2], at.xpeer)
+    ins.send_y(0, 0)
+    ins.send_y(0, 1)
+    ins.send_z(0, 1, FAR)
+    ins.send_z(0, 0, NEAR)
+    ins.send_z(0, 1, NEAR, at_end)
+    def half_block(p, n):
+        return x_ref.at[core, pl.ds(pl.multiple_of(p * rows + n * (rows // 2), rows // 2), rows // 2)]
+
+    def tok_z(n, p=p_own):
+        return remote(half_block(p, n), half_block(p, n), ts.at[1 + n], tr.at[1 + n], at.zpeer)
+
+    def tok_far(n, p=p_z):
+        return remote(half_block(p, n), half_block(p, n), ts.at[3 + n], tr.at[3 + n], at.xpeer)
+
+    def send_tok_z(n, only):
+        @pl.when(only)
+        def _():
+            tok_z(n).start()
+
+    tok_x = remote(block(p_own), block(p_own), ts.at[0], tr.at[0], at.xpeer)
     swaps = [
-        remote(tok_ref if k == 0 else block(p), block(p), ts.at[3 + k], tr.at[3 + k], at.partner)
+        remote(block(p), block(p), ts.at[5 + k], tr.at[5 + k], at.partner)
         for k, p in enumerate((p_own, p_x, p_z, p_far))
     ]
     tok_x.start()
-    tok_z.start()
+    send_tok_z(0, at_end)
     swaps[0].start()
     wbuf[zl, z, y, x] = w_ref[2 * zl + x]
-    x_ref[core, pl.ds(pl.multiple_of(p_own * rows, rows), rows), :] = tok_ref[...]
+    for load in loads[7:]:
+        load.wait()
+    join(raw[6:], o_ref)
+    obuf[zl, z, y, x] = o_ref[2 * zl + x]
     span = 2 * half // layers
     strip = 32
 
     def normalise(k, p):
-        remote(tok_ref, block(p, 1 - core), ts.at[3 + k], tr.at[3 + k], at.partner).wait_recv()
+        remote(block(p, core), block(p, 1 - core), ts.at[5 + k], tr.at[5 + k], at.partner).wait_recv()
 
         def step(i, carry):
             at_rows = pl.ds(pl.multiple_of(p * rows + i * strip, strip), strip)
@@ -396,38 +454,83 @@
         def _():
             add_layer(z + d, False)
 
-    ins.on_x()
-    ins.on_z(1, 0)
-    remote(tok_ref, block(p_z), ts.at[1], tr.at[1], at.zpeer).wait_recv()
-    tok_far.start()
+    def from_x(s):
+        ins.wait_x(s)
+        ins.send_z(1, s, FAR)
+        ins.send_z(1, s, NEAR, at_end)
+        ins.send_y(1, s)
+        ins.on_z(1, 0, s, FAR)
+
+    from_x(0)
+    send_tok_z(0, inside)
+    send_tok_z(1, at_end)
+    ins.on_z(1, 0, 0, NEAR, APART)
+    from_x(1)
+    send_tok_z(1, inside)
+    ins.send_z(0, 1, NEAR, inside)
+    for s in range(split):
+        ins.send_z(1, s, NEAR, inside)
+    normalise(0, p_own)
+    ins.on_z(1, 1, 0, FAR, PAIR, at_end)
+    ins.on_z(2, 0, 0, FAR, only=at_end)
+    ins.on_z(1, 1, 0, FAR, APART)
+    ins.on_z(2, 0, 0, FAR, only=inside)
+    ins.on_z(1, 1, 1, FAR, APART)
+    tok_z(0, p_z).wait_recv()
+    tok_far(0).start()
+    ins.on_z(2, 0, 1, FAR, only=inside)
+    ins.on_z(1, 1, 1, FAR, PAIR, at_end)
+    ins.on_z(1, 0, 1, NEAR, APART)
+    ins.on_z(1, 1, 0, FAR, PAIR, inside)
+    for s in range(split):
+        ins.on_z(1, 0, s, NEAR, PAIR)
+    remote(block(p_x), block(p_x), ts.at[0], tr.at[0], at.xpeer).wait_recv()
+    swaps[1].start()
+    ins.on_z(2, 0, 1, FAR, only=at_end)
+    ins.on_z(1, 1, 0, NEAR, APART)
+    normalise(1, p_x)
+    ins.on_z(1, 1, 1, NEAR, APART)
+    tok_z(1, p_z).wait_recv()
+    tok_far(1).start()
     swaps[2].start()
     outs.start_x()
-    remote(tok_ref, block(p_x), ts.at[0], tr.at[0], at.xpeer).wait_recv()
-    swaps[1].start()
-    ins.on_z(1, 1)
-    normalise(0, p_own)
+    ins.on_z(2, 1, 0, FAR, only=inside)
+    ins.on_z(2, 1, 0, FAR, only=at_end)
     normalise(2, p_z)
-    if layers > 2:
-        ins.on_z(2, 0)
-    normalise(1, p_x)
-    remote(tok_ref, block(p_far), ts.at[2], tr.at[2], at.xpeer).wait_recv()
+    ins.on_z(2, 0, 0, NEAR, only=inside)
+    ins.on_z(1, 1, 1, FAR, PAIR, inside)
+    for s in range(split):
+        ins.on_z(1, 1, s, NEAR, PAIR)
+    ins.on_z(3, 0, 0)
+    outs.send_z(0, 0, only=at_end)
+    ins.on_z(2, 0, 1, NEAR, only=inside)
+    tok_far(0, p_far).wait_recv()
+    tok_far(1, p_far).wait_recv()
     swaps[3].start()
-    if layers > 2:
-        ins.on_z(2, 1)
+    ins.on_z(2, 1, 1, FAR)
+    ins.on_z(3, 0, 1)
     normalise(3, p_far)
-    outs.start_z()
+    ins.on_z(2, 1, 0, NEAR, only=inside)
+    ins.on_z(3, 1, 0)
     ins.on_y(0)
     add_layer(z, True)
-    for d in range(3, layers):
-        ins.on_z(d, 0)
-        ins.on_z(d, 1)
+    ins.on_z(2, 1, 1, NEAR, only=inside)
+    outs.wait_x(0)
+    outs.on_z(1, 0, 0, FAR, PAIR, inside)
+    outs.send_z(0, 0, FAR, inside)
+    outs.send_z(1, 0, FAR)
+    outs.send_z(1, 0, NEAR, at_end)
+    outs.send_y(0, 0, inside)
+    outs.send_y(1, 0, inside)
+    ins.on_z(3, 1, 1)
     add_both(1)
-    outs.start_y()
-    outs.on_x()
-    obuf[zl, z, y, x] = o_ref[2 * zl + x]
-    for d in range(2, layers):
-        add_both(d)
-    outs.on_z(1, 0)
+    outs.send_y(0, 0, at_end)
+    outs.send_y(1, 0, at_end)
+    outs.on_z(1, 1, 0, FAR, PAIR, inside)
+    outs.on_z(2, 0, 0, FAR, only=inside)
+    add_both(2)
+    outs.on_z(1, 0, 0, FAR, APART)
+    add_both(3)
 
     def spread(i, carry):
         run, start = i // 4, pl.multiple_of(lax.rem(i, 4) * WINDOW, WINDOW)
@@ -466,6 +569,9 @@
             tails(1, 0, at.after, action)
 
     all_tails("start")
+    for r in range(2):
+        outs.on_z(1, r, 0, NEAR, PAIR)
+        outs.send_z(r, 0, NEAR, inside)
     first_run = (y == 0) & (zh == 0)
 
     @pl.when(first_run)
@@ -516,13 +622,15 @@
         mix(i, 0)
         return carry
 
+    for r in range(2):
+        outs.on_z(1, r, 0, FAR, PAIR, at_end)
+    outs.on_z(3, 0, 0)
+    outs.on_z(1, 1, 0, FAR, APART)
     lax.fori_loop(0, 3, inner_block, 0)
-    outs.on_z(1, 1)
-    if layers > 2:
-        outs.on_z(2, 0)
+    outs.on_z(2, 1, 0, FAR, only=inside)
+    outs.on_z(2, 0, 0, FAR, only=at_end)
     lax.fori_loop(3, 6, inner_block, 0)
-    if layers > 2:
-        outs.on_z(2, 1)
+    outs.on_z(2, 0, 0, NEAR, only=inside)
 
     def tails_in(after, target):
         for k, (ref, size) in enumerate(((ext, WINDOW), (gext, front))):
@@ -541,19 +649,20 @@
 
     tails_in(1, at.ypeer)
     lax.fori_loop(0, 2, first_block, 0)
-    for d in range(3, layers):
-        outs.on_z(d, 0)
-        outs.on_z(d, 1)
 
     lower = z < layers // 2
-    cols = obuf.shape[2] * obuf.shape[3] * obuf.shape[4]
-
-    def chunk_at(i):
-        return jnp.where(lower, i, layers - 1 - i)
-
-    def product(side, i):
+    cols = obuf.shape[3] * obuf.shape[4]
+    order = [(0, True), (1, True), (0, False), (1, False), (3, True), (2, True), (3, False), (2, False)]
+    chunks = len(order)
+
+    def chunk_at(h):
+        i, mine = order[h]
+        return jnp.where(lower, i, layers - 1 - i), y if mine else 1 - y
+
+    def product(side, h):
+        layer, row_y = chunk_at(h)
         return lax.dot_general(
-            hid[side], obuf[zl, chunk_at(i)].reshape(cols, hid.shape[2]),
+            hid[side], obuf[zl, layer, row_y].reshape(cols, hid.shape[2]),
             (((1,), (1,)), ((), ())), preferred_element_type=f32,
         )
 
@@ -594,46 +703,72 @@
         first_hop(i, 1).wait_recv()
         second_hop(i).wait_recv()
         total = s1[i, slab(p_own), :].astype(f32) + r1[i, 1].astype(f32) + r2[i].astype(f32)
-        out_ref[:, pl.ds(pl.multiple_of(chunk_at(i) * cols, cols), cols)] = total.astype(out_ref.dtype)
-
-    ready = -1
-    for i in range(layers):
-        need = max(i, layers // 2 - 1 - i)
-        while ready < need:
-            ready += 1
-            outs.on_y(ready)
-        begin(i)
-        if i > 0:
-            fold(i - 1)
-    fold(layers - 1)
-    for i in range(layers):
-        relay(i)
-    for i in range(layers):
-        collect(i)
-
-    ins.finish()
-    outs.finish()
-    all_tails("wait_send")
-    for copy in [tok_x, tok_z, tok_far] + swaps:
-        copy.wait_send()
-    for i in range(layers):
-        swap(i).wait_send()
-        first_hop(i, 0).wait_send()
-        first_hop(i, 1).wait_send()
-        second_hop(i).wait_send()
-
-
-def whole_layer(count, tokens, wblocks, oblocks, gain, taps, slopes, sinks, wide):
+        layer, row_y = chunk_at(i)
+        out_ref[:, pl.ds(pl.multiple_of((layer * 2 + row_y) * cols, cols), cols)] = total.astype(out_ref.dtype)
+
+    begin(0)
+    outs.on_z(1, 0, 0, NEAR, APART)
+    begin(1)
+    fold(0)
+    outs.on_z(2, 1, 0, FAR, only=at_end)
+    outs.on_y(0)
+    outs.on_y(1, sides=PAIR)
+    begin(2)
+    fold(1)
+    outs.on_z(1, 1, 0, NEAR, APART)
+    begin(3)
+    fold(2)
+    outs.on_z(2, 1, 0, NEAR, only=inside)
+    outs.on_z(3, 1, 0)
+    begin(4)
+    fold(3)
+    relay(0)
+    begin(5)
+    fold(4)
+    relay(1)
+    outs.on_y(2)
+    outs.on_y(3)
+    begin(6)
+    fold(5)
+    outs.on_y(1, sides=APART)
+    begin(7)
+    fold(6)
+    fold(7)
+    for h in range(2, chunks):
+        relay(h)
+        collect(h - 2)
+    for h in range(chunks - 2, chunks):
+        collect(h)
+
+    def phase_finish():
+        ins.finish()
+        outs.finish()
+        all_tails("wait_send")
+        for copy in [tok_x, tok_z(0), tok_z(1), tok_far(0), tok_far(1)] + swaps:
+            copy.wait_send()
+        for i in range(chunks):
+            swap(i).wait_send()
+            first_hop(i, 0).wait_send()
+            first_hop(i, 1).wait_send()
+            second_hop(i).wait_send()
+
+    phase_finish()
+
+
+def whole_layer(count, tokens, weights, gain, taps, slopes, sinks, wide):
     layers = count // PLANE
     rows, half = tokens.shape
-    _, depth, width = wblocks.shape
-    _, cols, inner = oblocks.shape
+    depth = weights[0].shape[0]
+    width = sum(w.shape[1] for w in weights[:6]) // PLANE
+    cols = weights[6].shape[0]
+    inner = sum(w.shape[1] for w in weights[6:]) // PLANE
     chans = taps.shape[1] // PLANE
     bf16, f32 = jnp.bfloat16, jnp.float32
     dma = pltpu.SemaphoreType.DMA
     split = 2
     length = 2 * rows
-    slab = 4 * cols
+    slab = 2 * cols
+    chunks = 2 * layers
 
     def sems(parts):
         hops = 2 * (layers - 1) * 4 * parts
@@ -642,11 +777,17 @@
     smem = pl.BlockSpec(memory_space=pltpu.SMEM)
     vmem = pl.BlockSpec(memory_space=pltpu.VMEM)
     return pl.pallas_call(
-        functools.partial(layer_kernel, count, chans, wide, split),
+        functools.partial(layer_entry, count, chans, wide, split),
         out_shape=jax.ShapeDtypeStruct((rows // 2, 2 * half), bf16),
-        in_specs=[smem] * 2 + [vmem] * 5,
+        in_specs=[smem] * 2 + [pl.BlockSpec(memory_space=pltpu.HBM)] * 11,
         out_specs=vmem,
-        scratch_shapes=[
+        scratch_shapes=[pltpu.VMEM(w.shape, bf16) for w in weights]
+        + [
+            pltpu.VMEM(gain.shape, f32),
+            pltpu.VMEM(taps.shape, f32),
+            pltpu.VMEM((PLANE, depth, width), bf16),
+            pltpu.VMEM((PLANE, cols, inner), bf16),
+            dma((11,)),
             pltpu.VMEM((2, PLANE * rows, half), bf16),
             pltpu.VMEM((layers, PLANE * rows, 2 * half // layers), bf16),
             pltpu.VMEM((2, layers, 2, 2, depth, width), bf16),
@@ -655,46 +796,25 @@
             pltpu.VMEM((2, WINDOW + length, 2 * HEAD), bf16),
             pltpu.VMEM((2, 8 + length, chans), f32),
             pltpu.VMEM((2, PLANE * WINDOW, inner), bf16),
-            pltpu.VMEM((layers, PLANE * WINDOW, slab), bf16),
-            pltpu.VMEM((layers, PLANE * WINDOW, slab), bf16),
+            pltpu.VMEM((chunks, PLANE * WINDOW, slab), bf16),
+            pltpu.VMEM((chunks, PLANE * WINDOW, slab), bf16),
             pltpu.VMEM((2, PLANE * WINDOW, slab), f32),
-            pltpu.VMEM((layers, PLANE * WINDOW, slab), bf16),
-            pltpu.VMEM((layers, 2, WINDOW, slab), bf16),
-            pltpu.VMEM((layers, WINDOW, slab), bf16),
-            pltpu.VMEM((layers, WINDOW, slab), bf16),
+            pltpu.VMEM((chunks, PLANE * WINDOW, slab), bf16),
+            pltpu.VMEM((chunks, 2, WINDOW, slab), bf16),
+            pltpu.VMEM((chunks, WINDOW, slab), bf16),
+            pltpu.VMEM((chunks, WINDOW, slab), bf16),
         ]
         + sems(split)
         + sems(1)
-        + [dma((7,))] * 2
+        + [dma((9,))] * 2
         + [dma((4,))] * 2
-        + [dma((layers,))] * 2
-        + [dma((2 * layers,))] * 2
-        + [dma((layers,))] * 2,
+        + [dma((chunks,))] * 2
+        + [dma((2 * chunks,))] * 2
+        + [dma((chunks,))] * 2,
         compiler_params=pltpu.CompilerParams(
             collective_id=0, has_side_effects=True, vmem_limit_bytes=60 << 20
         ),
-    )(slopes, sinks, tokens, wblocks, oblocks, gain, taps)
-
-
-def pack_kernel(*refs):
-    *weights, out_ref = refs
-    for p in range(PLANE):
-        pieces = []
-        for ref in weights:
-            width = ref.shape[1] // PLANE
-            pieces.append(ref[:, p * width : (p + 1) * width])
-        out_ref[p] = jnp.concatenate(pieces, axis=1)
-
-
-def pack(weights):
-    depth = weights[0].shape[0]
-    cols = sum(w.shape[1] for w in weights) // PLANE
-    return pl.pallas_call(
-        pack_kernel,
-        out_shape=jax.ShapeDtypeStruct((PLANE, depth, cols), weights[0].dtype),
-        in_specs=[pl.BlockSpec(memory_space=pltpu.VMEM)] * len(weights),
-        out_specs=pl.BlockSpec(memory_space=pltpu.VMEM),
-    )(*weights)
+    )(slopes, sinks, tokens, *weights, gain, taps)
 
 
 def plane_body(
@@ -717,22 +837,17 @@
             query_w, key_w, value_w, sink_logits, out_conv_w, out_attn_w,
         )
     count = lax.axis_size("sp")
-    chans = outer_gate_w.shape[1] // PLANE
     wide = query_w.shape[1] // PLANE
-    wblocks = pack((outer_gate_w, inner_gate_w, signal_w, query_w, key_w, value_w))
-    cols = out_conv_w.shape[1]
-    oblocks = jnp.concatenate(
-        [out_conv_w.reshape(PLANE, chans, cols), out_attn_w.reshape(PLANE, wide, cols)], axis=1
-    ).transpose(0, 2, 1)
+    weights = (outer_gate_w, inner_gate_w, signal_w, query_w, key_w, value_w, out_conv_w.T, out_attn_w.T)
     slopes = jnp.array([2.0 ** (-8.0 * h / QHEADS) for h in range(1, QHEADS + 1)], jnp.float32)
     return whole_layer(
-        count, tokens, wblocks, oblocks, norm_gain.reshape(1, -1), conv_taps, slopes, sink_logits, wide
+        count, tokens, weights, norm_gain.reshape(1, -1), conv_taps, slopes, sink_logits, wide
     )
 
 
 def solution(mesh):
     kv_local = KVHEADS // mesh.shape["tp"]
-    fits = mesh.shape["tp"] == 2 and kv_local == PLANE and mesh.shape["sp"] % (2 * PLANE) == 0
+    fits = mesh.shape["tp"] == 2 and kv_local == PLANE and mesh.shape["sp"] == LAYERS * PLANE
     chosen = plane_body if fits else body
     in_specs = (
         P("sp", "tp"),

time: 142 us -> 128 us (0.901)
  Pallas kernels: 137 us -> 125 us
  local copies, waits for them, and re-layouts: 3.89 us -> 2.06 us
    pallas_call x2 -> x1, Pallas kernels: 137 us -> 125 us  [whole_layer(): pl.pallas_call(functools.partial(layer_entry, count, chans, wide, split),...]
    reshape x4 -> x0, local copies, waits for them, and re-layouts: 1.82 us -> none  [the longest x2 1.43 us: plane_body(): out_conv_w.reshape(PLANE, chans, cols)]
where the time goes in v2:
time: 128 us; the launch traced here: 127 us
  Pallas kernels  125 us (98%)
  local copies, waits for them, and re-layouts  2.06 us (2%)
    pallas_call x1, Pallas kernels, whole_layer(): pl.pallas_call(functools.partial(layer_entry, count, chans, wide, split),...  125 us

profile of v2, /device:TPU:0, one launch (start us, length us, event | category | flops | bytes accessed | tf_op | source)
XLA Modules:
  0.0 127.3 jit_solution(10244004005058895661)
XLA Ops:
  0.0 125.3 %shard_map.127 = bf16[128,3072]{1,0:T(8,128)(2,1)} custom-call(f32[24]{0:T(128)} %constant.2.clone.slopes_ref, f32[12]{0:T(128)} %sinks_ref.1, bf16[256,1536]{1,0:T(8,128)(2,1)} %tok_hbm.1, bf16[192,768]{1,0:T(8,128)(2,1)} %refs_0_.1, bf16[192,768]{1,0:T(8,128)(2,1)} %refs_1_.1, bf16[192,768]{1,0:T(8,128)(2,1)} %refs_2_.1, bf16[192,768]{1,0:T(8,128)(2,1)} %refs_3_.1, ...), custom_call_target="tpu_custom_call" | custom-call | tf_op jit(solution)/shard_map/pallas_call | solution.py:779
  125.3 2.1 %copy.15 = bf16[128,3072]{1,0:T(8,128)(2,1)} copy(bf16[128,3072]{1,0:T(8,128)(2,1)} %shard_map.127) | data formatting | bytes 1572864

commit v3 on v2

--- a/solution.py
+++ b/solution.py
@@ -163,10 +163,11 @@
         at = self.at
         dst = self.slot(t, self.origin(up, d), at.y, self.column(r), s)
         src = self.src.at[2 * t + at.x, self.part(s)] if d == 0 and r == 0 else dst
-        i = ((((0 if up else 1) * (at.layers - 1) + send_d) * 2 + r) * 2 + t) * self.split + s
-        return remote(src, dst, self.zs.at[i], self.zr.at[i], at.above if up else at.below)
-
-    def z_send(self, up, d, r, t, s, action="start", only=True):
+        side = 0 if up else 1
+        i = (((side * (at.layers - 1) + send_d) * 2 + r) * 2 + t) * self.split + s
+        return remote(src, dst, self.zs.at[2 * side + t], self.zr.at[i], at.above if up else at.below)
+
+    def z_send(self, up, d, r, t, s, only=True):
         z, layers = self.at.z, self.at.layers
         if d >= layers - 1:
             return
@@ -177,22 +178,20 @@
 
         @pl.when(go & only)
         def _():
-            getattr(self.z_copy(up, d, r, t, s, d), action)()
+            self.z_copy(up, d, r, t, s, d).start()
 
     def y_copy(self, up, d, r, s, y):
         at = self.at
         dst = self.slot(at.zl, self.origin(up, d), y, self.column(r), s)
         src = self.src.at[2 * at.zl + at.x, self.part(s)] if d == 0 and r == 0 else dst
         m = d if up or d == 0 else at.layers - 1 + d
-        i = (m * 2 + r) * self.split + s
-        return remote(src, dst, self.ys.at[i], self.yr.at[i], at.ypeer)
+        return remote(src, dst, self.ys.at[0], self.yr.at[m], at.ypeer)
 
     def x_copy(self, t, s, receive=False):
         at = self.at
         src = self.src.at[2 * t + 1 - at.x, self.part(s)]
         dst = self.slot(t, at.z, at.y, 1 - at.x if receive else at.x, s)
-        i = t * self.split + s
-        return remote(src, dst, self.xs.at[i], self.xr.at[i], at.xpeer)
+        return remote(src, dst, self.xs.at[0], self.xr.at[t * self.split + s], at.xpeer)
 
     def send_z(self, r, s, which=FAR + NEAR, only=True):
         for k in which:
@@ -239,19 +238,17 @@
             arrive(True, 1 - k)
             arrive(False, k)
 
-    def on_y(self, d, action="wait_recv", sides=BOTH):
+    def on_y(self, d, sides=BOTH, up=None):
         z, layers, y, zl = self.at.z, self.at.layers, self.at.y, self.at.zl
-        side = 1 - y if action == "wait_recv" else y
 
         def each(up):
-            for r in range(2):
-                for s in range(self.split):
-                    getattr(self.y_copy(up, d, r, s, side), action)()
-
-        if d == 0:
-            each(True)
+            ref = self.buf.at[zl, self.origin(up, d), 1 - y]
+            m = d if up or d == 0 else layers - 1 + d
+            remote(ref, ref, self.ys.at[0], self.yr.at[m], self.at.ypeer).wait_recv()
+
+        if d == 0 or up is not None:
+            each(up is not False)
             return
-
         from_below, from_above = z >= d, z + d < layers
         if sides != BOTH:
             near = 1 if sides == PAIR else 0
@@ -266,16 +263,24 @@
             each(False)
 
     def finish(self):
-        for s in range(self.split):
+        at = self.at
+        layers = at.layers
+
+        def sent(ref, sem):
+            remote(ref, ref, sem, self.yr.at[0], at.ypeer).wait_send()
+
+        sent(self.buf.at[0, 0, 0], self.xs.at[0])
+        sent(self.buf.at[0, :, 0], self.ys.at[0])
+        for up in (True, False):
             for t in range(2):
-                self.x_copy(t, s).wait_send()
-        for d in range(self.at.layers):
-            self.on_y(d, "wait_send")
-            for r in range(2):
-                for t in range(2):
-                    for s in range(self.split):
-                        self.z_send(True, d, r, t, s, "wait_send")
-                        self.z_send(False, d, r, t, s, "wait_send")
+                for z in range(layers):
+                    beyond = layers - z if up else z + 1
+                    if beyond > (1 if (t == 1) == up else 2):
+                        number = z + 1 if up else layers - z
+
+                        @pl.when(at.z == z)
+                        def _():
+                            sent(self.buf.at[0, pl.ds(0, number), 0], self.zs.at[(0 if up else 2) + t])
 
 
 def join(weights, out_ref):
@@ -336,14 +341,14 @@
 def layer_entry(
     count, chans, wide, split, slopes_ref, sinks_ref, tok_hbm, *refs,
 ):
-    raw_hbm, (gain_hbm, taps_hbm, out_ref), refs = refs[:8], refs[8:11], refs[11:]
+    raw_hbm, (gain_hbm, taps_hbm, out_hbm), refs = refs[:8], refs[8:11], refs[11:]
     raw, refs = refs[:8], refs[8:]
-    layer_kernel(count, chans, wide, split, slopes_ref, sinks_ref, tok_hbm, raw_hbm, gain_hbm, taps_hbm, out_ref, raw, *refs)
+    layer_kernel(count, chans, wide, split, slopes_ref, sinks_ref, tok_hbm, raw_hbm, gain_hbm, taps_hbm, out_hbm, raw, *refs)
 
 
 def layer_kernel(
-    count, chans, wide, split, slopes_ref, sinks_ref, tok_hbm, raw_hbm, gain_hbm, taps_hbm, out_ref, raw,
-    gain_ref, taps_ref, w_ref, o_ref, ls, x_ref, nrm_ref, wbuf, obuf, acc_ref, ext, gext, hid, dsend, drecv, own, s1, r1, s2, r2,
+    count, chans, wide, split, slopes_ref, sinks_ref, tok_hbm, raw_hbm, gain_hbm, taps_hbm, out_hbm, raw,
+    gain_ref, taps_ref, w_ref, o_ref, out_ref, ls, os, x_ref, nrm_ref, wbuf, obuf, acc_ref, ext, gext, bias, hid, dsend, drecv, own, s1, r1, s2, r2,
     wzs, wzr, wys, wyr, wxs, wxr, ozs, ozr, oys, oyr, oxs, oxr, ts, tr, hs, hr, ds, dr, fs, fr, gs, gr,
 ):
     f32, bf16 = jnp.float32, jnp.bfloat16
@@ -390,10 +395,10 @@
         return x_ref.at[core, pl.ds(pl.multiple_of(p * rows + n * (rows // 2), rows // 2), rows // 2)]
 
     def tok_z(n, p=p_own):
-        return remote(half_block(p, n), half_block(p, n), ts.at[1 + n], tr.at[1 + n], at.zpeer)
+        return remote(half_block(p, n), half_block(p, n), ts.at[0], tr.at[1 + n], at.zpeer)
 
     def tok_far(n, p=p_z):
-        return remote(half_block(p, n), half_block(p, n), ts.at[3 + n], tr.at[3 + n], at.xpeer)
+        return remote(half_block(p, n), half_block(p, n), ts.at[0], tr.at[3 + n], at.xpeer)
 
     def send_tok_z(n, only):
         @pl.when(only)
@@ -402,11 +407,11 @@
 
     tok_x = remote(block(p_own), block(p_own), ts.at[0], tr.at[0], at.xpeer)
     swaps = [
-        remote(block(p), block(p), ts.at[5 + k], tr.at[5 + k], at.partner)
+        remote(block(p), block(p), ts.at[1], tr.at[5 + k], at.partner)
         for k, p in enumerate((p_own, p_x, p_z, p_far))
     ]
     tok_x.start()
-    send_tok_z(0, at_end)
+    tok_z(0).start()
     swaps[0].start()
     wbuf[zl, z, y, x] = w_ref[2 * zl + x]
     for load in loads[7:]:
@@ -417,7 +422,7 @@
     strip = 32
 
     def normalise(k, p):
-        remote(block(p, core), block(p, 1 - core), ts.at[5 + k], tr.at[5 + k], at.partner).wait_recv()
+        remote(block(p, core), block(p, 1 - core), ts.at[1], tr.at[5 + k], at.partner).wait_recv()
 
         def step(i, carry):
             at_rows = pl.ds(pl.multiple_of(p * rows + i * strip, strip), strip)
@@ -443,6 +448,34 @@
 
         lax.fori_loop(0, PLANE, step, 0)
 
+    def add_row(origin, row_y):
+        size = span // 2
+
+        def step(i, carry):
+            at_rows = pl.ds(pl.multiple_of(i * rows, rows), rows)
+            acc_ref[at_rows, :] += jnp.dot(
+                nrm_ref[origin, at_rows, pl.ds(pl.multiple_of(row_y * size, size), size)],
+                wbuf[zl, origin, row_y].reshape(size, wbuf.shape[5]),
+                preferred_element_type=f32,
+            )
+            return carry
+
+        lax.fori_loop(0, PLANE, step, 0)
+
+    def add_last():
+        def two(d, up):
+            add_row(ins.origin(up, d), y)
+            ins.on_y(d, up=up)
+            add_row(ins.origin(up, d), 1 - y)
+
+        for above in (False, True):
+            for d, where in ((3, at_end), (2, inside)):
+                mine = (z >= d) if above else (z + d < layers)
+
+                @pl.when(mine & where)
+                def _():
+                    two(d, above)
+
     def add_both(d):
         ins.on_y(d)
 
@@ -462,7 +495,6 @@
         ins.on_z(1, 0, s, FAR)
 
     from_x(0)
-    send_tok_z(0, inside)
     send_tok_z(1, at_end)
     ins.on_z(1, 0, 0, NEAR, APART)
     from_x(1)
@@ -470,6 +502,7 @@
     ins.send_z(0, 1, NEAR, inside)
     for s in range(split):
         ins.send_z(1, s, NEAR, inside)
+    outs.send_y(0, 0, inside)
     normalise(0, p_own)
     ins.on_z(1, 1, 0, FAR, PAIR, at_end)
     ins.on_z(2, 0, 0, FAR, only=at_end)
@@ -487,6 +520,7 @@
     remote(block(p_x), block(p_x), ts.at[0], tr.at[0], at.xpeer).wait_recv()
     swaps[1].start()
     ins.on_z(2, 0, 1, FAR, only=at_end)
+    outs.send_y(0, 0, at_end)
     ins.on_z(1, 1, 0, NEAR, APART)
     normalise(1, p_x)
     ins.on_z(1, 1, 1, NEAR, APART)
@@ -520,17 +554,19 @@
     outs.send_z(0, 0, FAR, inside)
     outs.send_z(1, 0, FAR)
     outs.send_z(1, 0, NEAR, at_end)
-    outs.send_y(0, 0, inside)
     outs.send_y(1, 0, inside)
     ins.on_z(3, 1, 1)
     add_both(1)
-    outs.send_y(0, 0, at_end)
     outs.send_y(1, 0, at_end)
     outs.on_z(1, 1, 0, FAR, PAIR, inside)
     outs.on_z(2, 0, 0, FAR, only=inside)
-    add_both(2)
+
+    @pl.when(at_end)
+    def _():
+        add_both(2)
+
     outs.on_z(1, 0, 0, FAR, APART)
-    add_both(3)
+    add_last()
 
     def spread(i, carry):
         run, start = i // 4, pl.multiple_of(lax.rem(i, 4) * WINDOW, WINDOW)
@@ -586,7 +622,11 @@
     near = (dist >= 0) & (dist < WINDOW)
     far = dist.astype(f32)
 
-    def mix(run, blk):
+    for g in range(group):
+        bias[g] = jnp.where(near, -slopes_ref[(core * PLANE + spot) * group + g] * far, -1e30)
+    ones = jnp.where(lax.broadcasted_iota(jnp.int32, (2 * WINDOW, HEAD), 1) == 0, 1.0, 0.0).astype(bf16)
+
+    def mix(run, blk, first=False):
         start = pl.multiple_of(blk * WINDOW, WINDOW)
         chunk = acc_ref[pl.ds(pl.multiple_of(run * length + start, WINDOW), WINDOW), :].astype(bf16)
         window = gext[run, pl.ds(start, WINDOW + front), :]
@@ -596,41 +636,40 @@
         )
         pieces = [(chunk[:, :chans].astype(f32) * conv).astype(bf16)]
         kv = ext[run, pl.ds(start, 2 * WINDOW), :]
-        keys, values = kv[:, :HEAD], kv[:, HEAD:]
+        keys, values = kv[:, :HEAD], jnp.concatenate([kv[:, HEAD:], ones], axis=1)
         offset = ((2 * zh + run) * 2 + y) * length
-        valid = near & (offset + start - WINDOW + col >= 0)
         for g in range(group):
-            first = 3 * chans + g * HEAD
-            scores = lax.dot_general(
-                chunk[:, first : first + HEAD], keys, (((1,), (1,)), ((), ())), preferred_element_type=f32
-            ) * HEAD ** (-0.5)
-            scores = jnp.where(valid, scores - slopes_ref[(core * PLANE + spot) * group + g] * far, -1e30)
+            at_head = 3 * chans + g * HEAD
+            query = chunk[:, at_head : at_head + HEAD] * jnp.asarray(HEAD ** (-0.5), bf16)
+            scores = bias[g] + lax.dot_general(
+                query, keys, (((1,), (1,)), ((), ())), preferred_element_type=f32
+            )
+            if first:
+                scores = jnp.where(offset - WINDOW + col >= 0, scores, -1e30)
             sink = sinks_ref[spot * group + g]
             top = jnp.maximum(jnp.max(scores, axis=1, keepdims=True), sink)
-            expo = jnp.exp(scores - top)
-            total = jnp.sum(expo, axis=1, keepdims=True) + jnp.exp(sink - top)
-            probs = (expo / total).astype(bf16)
-            pieces.append(jnp.dot(probs, values, preferred_element_type=f32).astype(bf16))
+            expo = jnp.exp(scores - top).astype(bf16)
+            summed = jnp.dot(expo, values, preferred_element_type=f32)
+            total = summed[:, HEAD : HEAD + 1] + jnp.exp(sink - top)
+            pieces.append((summed[:, :HEAD] / total).astype(bf16))
         place = pl.ds(pl.multiple_of((2 * run + blk // 2) * WINDOW, WINDOW), WINDOW)
         hid[lax.rem(blk, 2), place, :] = jnp.concatenate(pieces, axis=1)
 
-    def inner_block(i, carry):
-        mix(i // 3, 1 + lax.rem(i, 3))
-        return carry
-
-    def first_block(i, carry):
-        mix(i, 0)
-        return carry
+    def mix_run(run):
+        for blk in range(1, 4):
+            mix(run, blk)
+
+    def mix_first():
+        for run in range(2):
+            mix(run, 0, True)
 
     for r in range(2):
         outs.on_z(1, r, 0, FAR, PAIR, at_end)
     outs.on_z(3, 0, 0)
     outs.on_z(1, 1, 0, FAR, APART)
-    lax.fori_loop(0, 3, inner_block, 0)
+    mix_run(0)
     outs.on_z(2, 1, 0, FAR, only=inside)
-    outs.on_z(2, 0, 0, FAR, only=at_end)
-    lax.fori_loop(3, 6, inner_block, 0)
-    outs.on_z(2, 0, 0, NEAR, only=inside)
+    mix_run(1)
 
     def tails_in(after, target):
         for k, (ref, size) in enumerate(((ext, WINDOW), (gext, front))):
@@ -648,7 +687,7 @@
         tails_in(0, at.prior)
 
     tails_in(1, at.ypeer)
-    lax.fori_loop(0, 2, first_block, 0)
+    mix_first()
 
     lower = z < layers // 2
     cols = obuf.shape[3] * obuf.shape[4]
@@ -670,17 +709,17 @@
         return pl.ds(pl.multiple_of(p * WINDOW, WINDOW), WINDOW)
 
     def swap(i):
-        return remote(dsend.at[i], drecv.at[i], ds.at[i], dr.at[i], at.partner)
+        return remote(dsend.at[i], drecv.at[i], ds.at[0], dr.at[i], at.partner)
 
     def first_hop(i, j):
         if i % 2 == 0:
             target, p = at.xpeer, (2 * (1 - zl) if j == 0 else 2 * zl) + 1 - x
         else:
             target, p = at.zpeer, 2 * (1 - zl) + ((1 - x) if j == 0 else x)
-        return remote(s1.at[i, slab(p)], r1.at[i, j], fs.at[2 * i + j], fr.at[2 * i + j], target)
+        return remote(s1.at[i, slab(p)], r1.at[i, j], fs.at[0], fr.at[2 * i + j], target)
 
     def second_hop(i):
-        return remote(s2.at[i], r2.at[i], gs.at[i], gr.at[i], at.zpeer if i % 2 == 0 else at.xpeer)
+        return remote(s2.at[i], r2.at[i], gs.at[0], gr.at[i], at.zpeer if i % 2 == 0 else at.xpeer)
 
     def begin(i):
         dsend[i] = product(1 - core, i).astype(bf16)
@@ -699,17 +738,25 @@
         s2[i] = (s1[i, slab(p), :].astype(f32) + r1[i, 0].astype(f32)).astype(bf16)
         second_hop(i).start()
 
+    def out_copy(i):
+        layer, row_y = chunk_at(i)
+        return pltpu.make_async_copy(
+            out_ref.at[i], out_hbm.at[:, pl.ds(pl.multiple_of((layer * 2 + row_y) * cols, cols), cols)], os.at[0]
+        )
+
     def collect(i):
         first_hop(i, 1).wait_recv()
         second_hop(i).wait_recv()
         total = s1[i, slab(p_own), :].astype(f32) + r1[i, 1].astype(f32) + r2[i].astype(f32)
-        layer, row_y = chunk_at(i)
-        out_ref[:, pl.ds(pl.multiple_of((layer * 2 + row_y) * cols, cols), cols)] = total.astype(out_ref.dtype)
+        out_ref[i] = total.astype(out_ref.dtype)
+        out_copy(i).start()
 
     begin(0)
-    outs.on_z(1, 0, 0, NEAR, APART)
+    outs.on_z(2, 0, 0, FAR, only=at_end)
     begin(1)
     fold(0)
+    outs.on_z(2, 0, 0, NEAR, only=inside)
+    outs.on_z(1, 0, 0, NEAR, APART)
     outs.on_z(2, 1, 0, FAR, only=at_end)
     outs.on_y(0)
     outs.on_y(1, sides=PAIR)
@@ -726,6 +773,8 @@
     begin(5)
     fold(4)
     relay(1)
+    relay(2)
+    relay(3)
     outs.on_y(2)
     outs.on_y(3)
     begin(6)
@@ -733,24 +782,31 @@
     outs.on_y(1, sides=APART)
     begin(7)
     fold(6)
+    relay(4)
     fold(7)
-    for h in range(2, chunks):
-        relay(h)
-        collect(h - 2)
-    for h in range(chunks - 2, chunks):
+    collect(0)
+    collect(1)
+    relay(5)
+    collect(2)
+    relay(6)
+    collect(3)
+    relay(7)
+    for h in range(4, chunks):
         collect(h)
 
     def phase_finish():
+        pltpu.make_async_copy(out_ref, out_ref, os.at[0]).wait()
         ins.finish()
         outs.finish()
         all_tails("wait_send")
-        for copy in [tok_x, tok_z(0), tok_z(1), tok_far(0), tok_far(1)] + swaps:
-            copy.wait_send()
-        for i in range(chunks):
-            swap(i).wait_send()
-            first_hop(i, 0).wait_send()
-            first_hop(i, 1).wait_send()
-            second_hop(i).wait_send()
+        for ref, sem in (
+            (x_ref.at[0, pl.ds(0, 3 * rows)], ts.at[0]),
+            (x_ref.at[0], ts.at[1]),
+            (dsend, ds.at[0]),
+            (s1.at[pl.ds(0, chunks // 2)], fs.at[0]),
+            (s2, gs.at[0]),
+        ):
+            remote(ref, ref, sem, dr.at[0], at.partner).wait_send()
 
     phase_finish()
 
@@ -772,22 +828,23 @@
 
     def sems(parts):
         hops = 2 * (layers - 1) * 4 * parts
-        return [dma((hops,))] * 2 + [dma(((2 * layers - 1) * 2 * parts,))] * 2 + [dma((2 * parts,))] * 2
+        return [dma((number,)) for number in (4, hops, 1, 2 * layers - 1, 1, 2 * parts)]
 
     smem = pl.BlockSpec(memory_space=pltpu.SMEM)
-    vmem = pl.BlockSpec(memory_space=pltpu.VMEM)
     return pl.pallas_call(
         functools.partial(layer_entry, count, chans, wide, split),
         out_shape=jax.ShapeDtypeStruct((rows // 2, 2 * half), bf16),
         in_specs=[smem] * 2 + [pl.BlockSpec(memory_space=pltpu.HBM)] * 11,
-        out_specs=vmem,
+        out_specs=pl.BlockSpec(memory_space=pltpu.HBM),
         scratch_shapes=[pltpu.VMEM(w.shape, bf16) for w in weights]
         + [
             pltpu.VMEM(gain.shape, f32),
             pltpu.VMEM(taps.shape, f32),
             pltpu.VMEM((PLANE, depth, width), bf16),
             pltpu.VMEM((PLANE, cols, inner), bf16),
+            pltpu.VMEM((chunks, WINDOW, slab), bf16),
             dma((11,)),
+            dma((1,)),
             pltpu.VMEM((2, PLANE * rows, half), bf16),
             pltpu.VMEM((layers, PLANE * rows, 2 * half // layers), bf16),
             pltpu.VMEM((2, layers, 2, 2, depth, width), bf16),
@@ -795,6 +852,7 @@
             pltpu.VMEM((PLANE * rows, width), f32),
             pltpu.VMEM((2, WINDOW + length, 2 * HEAD), bf16),
             pltpu.VMEM((2, 8 + length, chans), f32),
+            pltpu.VMEM((QHEADS // KVHEADS, WINDOW, 2 * WINDOW), f32),
             pltpu.VMEM((2, PLANE * WINDOW, inner), bf16),
             pltpu.VMEM((chunks, PLANE * WINDOW, slab), bf16),
             pltpu.VMEM((chunks, PLANE * WINDOW, slab), bf16),
@@ -806,11 +864,7 @@
         ]
         + sems(split)
         + sems(1)
-        + [dma((9,))] * 2
-        + [dma((4,))] * 2
-        + [dma((chunks,))] * 2
-        + [dma((2 * chunks,))] * 2
-        + [dma((chunks,))] * 2,
+        + [dma((number,)) for number in (2, 9, 4, 4, 1, chunks, 1, 2 * chunks, 1, chunks)],
         compiler_params=pltpu.CompilerParams(
             collective_id=0, has_side_effects=True, vmem_limit_bytes=60 << 20
         ),

time: 128 us -> 122 us (0.953)
  Pallas kernels: 125 us -> 119 us
    pallas_call x1, Pallas kernels: 125 us -> 119 us  [whole_layer(): pl.pallas_call(functools.partial(layer_entry, count, chans, wide, split),...]
where the time goes in v3:
time: 122 us
  Pallas kernels  119 us (98%)
  local copies, waits for them, and re-layouts  2.06 us (2%)
    pallas_call x1, Pallas kernels, whole_layer(): pl.pallas_call(functools.partial(layer_entry, count, chans, wide, split),...  119 us

profile of v3, /device:TPU:0, one launch (start us, length us, event | category | flops | bytes accessed | tf_op | source)
XLA Modules:
  0.0 121.6 jit_solution(10860855616804765497)
XLA Ops:
  0.0 119.5 %shard_map.127 = bf16[128,3072]{1,0:T(8,128)(2,1)} custom-call(f32[24]{0:T(128)} %constant.2.clone.slopes_ref, f32[12]{0:T(128)} %sinks_ref.1, bf16[256,1536]{1,0:T(8,128)(2,1)} %tok_hbm.1, bf16[192,768]{1,0:T(8,128)(2,1)} %refs_0_.1, bf16[192,768]{1,0:T(8,128)(2,1)} %refs_1_.1, bf16[192,768]{1,0:T(8,128)(2,1)} %refs_2_.1, bf16[192,768]{1,0:T(8,128)(2,1)} %refs_3_.1, ...), custom_call_target="tpu_custom_call" | custom-call | tf_op jit(solution)/shard_map/pallas_call | solution.py:834
  119.5 2.1 %copy.15 = bf16[128,3072]{1,0:T(8,128)(2,1)} copy(bf16[128,3072]{1,0:T(8,128)(2,1)} %shard_map.127) | data formatting | bytes 1572864

commit v4 on v3

--- a/solution.py
+++ b/solution.py
@@ -341,14 +341,14 @@
 def layer_entry(
     count, chans, wide, split, slopes_ref, sinks_ref, tok_hbm, *refs,
 ):
-    raw_hbm, (gain_hbm, taps_hbm, out_hbm), refs = refs[:8], refs[8:11], refs[11:]
+    raw_hbm, (gain_hbm, taps_hbm, out_hbm, far_hbm), refs = refs[:8], refs[8:12], refs[12:]
     raw, refs = refs[:8], refs[8:]
-    layer_kernel(count, chans, wide, split, slopes_ref, sinks_ref, tok_hbm, raw_hbm, gain_hbm, taps_hbm, out_hbm, raw, *refs)
+    layer_kernel(count, chans, wide, split, slopes_ref, sinks_ref, tok_hbm, raw_hbm, gain_hbm, taps_hbm, out_hbm, far_hbm, raw, *refs)
 
 
 def layer_kernel(
-    count, chans, wide, split, slopes_ref, sinks_ref, tok_hbm, raw_hbm, gain_hbm, taps_hbm, out_hbm, raw,
-    gain_ref, taps_ref, w_ref, o_ref, out_ref, ls, os, x_ref, nrm_ref, wbuf, obuf, acc_ref, ext, gext, bias, hid, dsend, drecv, own, s1, r1, s2, r2,
+    count, chans, wide, split, slopes_ref, sinks_ref, tok_hbm, raw_hbm, gain_hbm, taps_hbm, out_hbm, far_hbm, raw,
+    gain_ref, taps_ref, w_ref, o_ref, out_ref, ls, os, x_ref, nrm_ref, wbuf, obuf, acc_ref, ext, gext, bias, hid, dsend, drecv, own, s1, r1, s2,
     wzs, wzr, wys, wyr, wxs, wxr, ozs, ozr, oys, oyr, oxs, oxr, ts, tr, hs, hr, ds, dr, fs, fr, gs, gr,
 ):
     f32, bf16 = jnp.float32, jnp.bfloat16
@@ -718,8 +718,12 @@
             target, p = at.zpeer, 2 * (1 - zl) + ((1 - x) if j == 0 else x)
         return remote(s1.at[i, slab(p)], r1.at[i, j], fs.at[0], fr.at[2 * i + j], target)
 
+    def out_slab(i):
+        layer, row_y = chunk_at(i)
+        return pl.ds(pl.multiple_of((layer * 2 + row_y) * cols, cols), cols)
+
     def second_hop(i):
-        return remote(s2.at[i], r2.at[i], gs.at[0], gr.at[i], at.zpeer if i % 2 == 0 else at.xpeer)
+        return remote(s2.at[i], far_hbm.at[:, out_slab(i)], gs.at[0], gr.at[i], at.zpeer if i % 2 == 0 else at.xpeer)
 
     def begin(i):
         dsend[i] = product(1 - core, i).astype(bf16)
@@ -739,15 +743,11 @@
         second_hop(i).start()
 
     def out_copy(i):
-        layer, row_y = chunk_at(i)
-        return pltpu.make_async_copy(
-            out_ref.at[i], out_hbm.at[:, pl.ds(pl.multiple_of((layer * 2 + row_y) * cols, cols), cols)], os.at[0]
-        )
+        return pltpu.make_async_copy(out_ref.at[i], out_hbm.at[:, out_slab(i)], os.at[0])
 
     def collect(i):
         first_hop(i, 1).wait_recv()
-        second_hop(i).wait_recv()
-        total = s1[i, slab(p_own), :].astype(f32) + r1[i, 1].astype(f32) + r2[i].astype(f32)
+        total = s1[i, slab(p_own), :].astype(f32) + r1[i, 1].astype(f32)
         out_ref[i] = total.astype(out_ref.dtype)
         out_copy(i).start()
 
@@ -755,47 +755,46 @@
     outs.on_z(2, 0, 0, FAR, only=at_end)
     begin(1)
     fold(0)
+    fold(1)
+    outs.on_z(2, 1, 0, FAR, only=at_end)
     outs.on_z(2, 0, 0, NEAR, only=inside)
-    outs.on_z(1, 0, 0, NEAR, APART)
-    outs.on_z(2, 1, 0, FAR, only=at_end)
     outs.on_y(0)
     outs.on_y(1, sides=PAIR)
     begin(2)
-    fold(1)
-    outs.on_z(1, 1, 0, NEAR, APART)
+    outs.on_z(1, 0, 0, NEAR, APART)
+    outs.on_z(3, 1, 0)
     begin(3)
     fold(2)
+    fold(3)
+    outs.on_z(1, 1, 0, NEAR, APART)
+    relay(0)
     outs.on_z(2, 1, 0, NEAR, only=inside)
-    outs.on_z(3, 1, 0)
     begin(4)
-    fold(3)
-    relay(0)
+    relay(1)
     begin(5)
     fold(4)
-    relay(1)
+    fold(5)
+    collect(0)
+    collect(1)
     relay(2)
     relay(3)
     outs.on_y(2)
     outs.on_y(3)
     begin(6)
-    fold(5)
     outs.on_y(1, sides=APART)
     begin(7)
     fold(6)
-    relay(4)
     fold(7)
-    collect(0)
-    collect(1)
-    relay(5)
     collect(2)
-    relay(6)
     collect(3)
-    relay(7)
     for h in range(4, chunks):
+        relay(h)
         collect(h)
 
     def phase_finish():
         pltpu.make_async_copy(out_ref, out_ref, os.at[0]).wait()
+        for h in range(chunks):
+            second_hop(h).wait_recv()
         ins.finish()
         outs.finish()
         all_tails("wait_send")
@@ -833,9 +832,9 @@
     smem = pl.BlockSpec(memory_space=pltpu.SMEM)
     return pl.pallas_call(
         functools.partial(layer_entry, count, chans, wide, split),
-        out_shape=jax.ShapeDtypeStruct((rows // 2, 2 * half), bf16),
+        out_shape=[jax.ShapeDtypeStruct((rows // 2, 2 * half), bf16)] * 2,
         in_specs=[smem] * 2 + [pl.BlockSpec(memory_space=pltpu.HBM)] * 11,
-        out_specs=pl.BlockSpec(memory_space=pltpu.HBM),
+        out_specs=[pl.BlockSpec(memory_space=pltpu.HBM)] * 2,
         scratch_shapes=[pltpu.VMEM(w.shape, bf16) for w in weights]
         + [
             pltpu.VMEM(gain.shape, f32),
@@ -860,7 +859,6 @@
             pltpu.VMEM((chunks, PLANE * WINDOW, slab), bf16),
             pltpu.VMEM((chunks, 2, WINDOW, slab), bf16),
             pltpu.VMEM((chunks, WINDOW, slab), bf16),
-            pltpu.VMEM((chunks, WINDOW, slab), bf16),
         ]
         + sems(split)
         + sems(1)
@@ -894,9 +892,10 @@
     wide = query_w.shape[1] // PLANE
     weights = (outer_gate_w, inner_gate_w, signal_w, query_w, key_w, value_w, out_conv_w.T, out_attn_w.T)
     slopes = jnp.array([2.0 ** (-8.0 * h / QHEADS) for h in range(1, QHEADS + 1)], jnp.float32)
-    return whole_layer(
+    near, far = whole_layer(
         count, tokens, weights, norm_gain.reshape(1, -1), conv_taps, slopes, sink_logits, wide
     )
+    return (near.astype(jnp.float32) + far.astype(jnp.float32)).astype(jnp.bfloat16)
 
 
 def solution(mesh):

time: 122 us -> 118 us (0.967)
  Pallas kernels: 119 us -> 115 us
  other arithmetic: 0 us -> 2.44 us
  local copies, waits for them, and re-layouts: 2.06 us -> 0 us
    pallas_call x1, Pallas kernels: 119 us -> 115 us  [whole_layer(): pl.pallas_call(functools.partial(layer_entry, count, chans, wide, split),...]
    convert_element_type x0 -> x1, other arithmetic: none -> 2.44 us  [plane_body(): (near.astype(jnp.float32) + far.astype(jnp.float32)).astype(jnp.bfloat16)]
    unnamed x1 -> x0, local copies, waits for them, and re-layouts: 2.06 us -> none
where the time goes in v4:
time: 118 us
  Pallas kernels  115 us (97%)
  other arithmetic  2.44 us (2%)
    pallas_call x1, Pallas kernels, whole_layer(): pl.pallas_call(functools.partial(layer_entry, count, chans, wide, split),...  115 us
    convert_element_type x1, other arithmetic, plane_body(): (near.astype(jnp.float32) + far.astype(jnp.float32)).astype(jnp.bfloat16)  2.44 us

profile of v4, /device:TPU:0, one launch (start us, length us, event | category | flops | bytes accessed | tf_op | source)
XLA Modules:
  0.0 117.8 jit_solution(6593410730954883475)
XLA Ops:
  0.0 115.3 %shard_map.127 = (bf16[128,3072]{1,0:T(8,128)(2,1)}, bf16[128,3072]{1,0:T(8,128)(2,1)}) custom-call(f32[24]{0:T(128)} %constant.2.clone.slopes_ref, f32[12]{0:T(128)} %sinks_ref.1, bf16[256,1536]{1,0:T(8,128)(2,1)} %tok_hbm.1, bf16[192,768]{1,0:T(8,128)(2,1)} %refs_0_.1, bf16[192,768]{1,0:T(8,128)(2,1)} %refs_1_.1, bf16[192,768]{1,0:T(8,128)(2,1)} %refs_2_.1, ...), custom_call_target="tpu_custom_call" | custom-call | tf_op jit(solution)/shard_map/pallas_call | solution.py:833
  115.4 2.4 %add_convert_fusion = bf16[128,3072]{1,0:T(8,128)(2,1)} fusion(bf16[128,3072]{1,0:T(8,128)(2,1)} %get-tuple-element.8, bf16[128,3072]{1,0:T(8,128)(2,1)} %get-tuple-element.7), kind=kLoop, calls=%fused_computation | loop fusion | flops 1572864 | bytes 2359296 | tf_op jit(solution)/shard_map/convert_element_type | solution.py:898

commit v5 on v4

--- a/solution.py
+++ b/solution.py
@@ -448,11 +448,11 @@
 
         lax.fori_loop(0, PLANE, step, 0)
 
-    def add_row(origin, row_y):
+    def add_row(origin, row_y, first=0, stride=1):
         size = span // 2
 
         def step(i, carry):
-            at_rows = pl.ds(pl.multiple_of(i * rows, rows), rows)
+            at_rows = pl.ds(pl.multiple_of((first + stride * i) * rows, rows), rows)
             acc_ref[at_rows, :] += jnp.dot(
                 nrm_ref[origin, at_rows, pl.ds(pl.multiple_of(row_y * size, size), size)],
                 wbuf[zl, origin, row_y].reshape(size, wbuf.shape[5]),
@@ -460,13 +460,16 @@
             )
             return carry
 
-        lax.fori_loop(0, PLANE, step, 0)
-
-    def add_last():
+        lax.fori_loop(0, PLANE // stride, step, 0)
+
+    def add_last(rest=False):
         def two(d, up):
+            if rest:
+                add_row(ins.origin(up, d), 1 - y, 0, 2)
+                return
             add_row(ins.origin(up, d), y)
             ins.on_y(d, up=up)
-            add_row(ins.origin(up, d), 1 - y)
+            add_row(ins.origin(up, d), 1 - y, 1, 2)
 
         for above in (False, True):
             for d, where in ((3, at_end), (2, inside)):
@@ -568,15 +571,18 @@
     outs.on_z(1, 0, 0, FAR, APART)
     add_last()
 
-    def spread(i, carry):
-        run, start = i // 4, pl.multiple_of(lax.rem(i, 4) * WINDOW, WINDOW)
-        chunk = acc_ref[pl.ds(pl.multiple_of(i * WINDOW, WINDOW), WINDOW), :].astype(bf16)
-        ext[run, pl.ds(start + WINDOW, WINDOW), :] = chunk[:, 3 * chans + wide :]
-        product = chunk[:, chans : 2 * chans].astype(f32) * chunk[:, 2 * chans : 3 * chans].astype(f32)
-        gext[run, pl.ds(start + front, WINDOW), :] = product.astype(bf16).astype(f32)
-        return carry
-
-    lax.fori_loop(0, 2 * length // WINDOW, spread, 0)
+    blocks = 2 * length // WINDOW
+
+    def mix_spread(some):
+        for i in some:
+            run, start = i // 4, i % 4 * WINDOW
+            here = pl.ds(i * WINDOW, WINDOW)
+            ext[run, pl.ds(start + WINDOW, WINDOW), :] = acc_ref[here, 3 * chans + wide :].astype(bf16)
+            both = acc_ref[here, chans : 3 * chans].astype(bf16).astype(f32)
+            gext[run, pl.ds(start + front, WINDOW), :] = (both[:, :chans] * both[:, chans:]).astype(bf16).astype(f32)
+
+    tail_blocks = range(blocks // 2 - 1, blocks, blocks // 2)
+    mix_spread(tail_blocks)
 
     def tails(run, after, target, action):
         kv = remote(
@@ -605,6 +611,11 @@
             tails(1, 0, at.after, action)
 
     all_tails("start")
+    for r in range(2):
+        outs.on_z(1, r, 0, FAR, PAIR, at_end)
+    add_last(True)
+    mix_spread([i for i in range(blocks) if i not in tail_blocks])
+    outs.on_z(3, 0, 0)
     for r in range(2):
         outs.on_z(1, r, 0, NEAR, PAIR)
         outs.send_z(r, 0, NEAR, inside)
@@ -663,9 +674,6 @@
         for run in range(2):
             mix(run, 0, True)
 
-    for r in range(2):
-        outs.on_z(1, r, 0, FAR, PAIR, at_end)
-    outs.on_z(3, 0, 0)
     outs.on_z(1, 1, 0, FAR, APART)
     mix_run(0)
     outs.on_z(2, 1, 0, FAR, only=inside)
@@ -869,6 +877,18 @@
     )(slopes, sinks, tokens, *weights, gain, taps)
 
 
+def add_kernel(a_ref, b_ref, out_ref):
+    out_ref[...] = (a_ref[...].astype(jnp.float32) + b_ref[...].astype(jnp.float32)).astype(out_ref.dtype)
+
+
+def add_pair(a, b):
+    rows, cols = a.shape
+    spec = pl.BlockSpec((rows // 2, cols), lambda i: (i, 0))
+    return pl.pallas_call(
+        add_kernel, grid=(2,), in_specs=[spec] * 2, out_specs=spec, out_shape=jax.ShapeDtypeStruct(a.shape, a.dtype)
+    )(a, b)
+
+
 def plane_body(
     tokens,
     norm_gain,
@@ -895,7 +915,7 @@
     near, far = whole_layer(
         count, tokens, weights, norm_gain.reshape(1, -1), conv_taps, slopes, sink_logits, wide
     )
-    return (near.astype(jnp.float32) + far.astype(jnp.float32)).astype(jnp.bfloat16)
+    return add_pair(near, far)
 
 
 def solution(mesh):

time: 118 us -> 116 us (0.983)
  other arithmetic: 2.44 us -> 0 us
    convert_element_type x1 -> x0, other arithmetic: 2.44 us -> none  [plane_body(): (near.astype(jnp.float32) + far.astype(jnp.float32)).astype(jnp.bfloat16)]
    pallas_call x0 -> x1, Pallas kernels: none -> 2.21 us  [add_pair(): pl.pallas_call(add_kernel, grid=(2,), in_specs=[spec] * 2, out_specs=spec...]
    pallas_call x1, Pallas kernels: 115 us -> 114 us  [whole_layer(): pl.pallas_call(functools.partial(layer_entry, count, chans, wide, split),...]
where the time goes in v5:
time: 116 us
  Pallas kernels  116 us (100%)
    pallas_call x1, Pallas kernels, whole_layer(): pl.pallas_call(functools.partial(layer_entry, count, chans, wide, split),...  114 us

profile of v5, /device:TPU:0, one launch (start us, length us, event | category | flops | bytes accessed | tf_op | source)
XLA Modules:
  0.0 115.7 jit_solution(11576356704938322165)
XLA Ops:
  0.0 113.5 %shard_map.127 = (bf16[128,3072]{1,0:T(8,128)(2,1)}, bf16[128,3072]{1,0:T(8,128)(2,1)}) custom-call(f32[24]{0:T(128)} %constant.2.clone.slopes_ref, f32[12]{0:T(128)} %sinks_ref.1, bf16[256,1536]{1,0:T(8,128)(2,1)} %tok_hbm.1, bf16[192,768]{1,0:T(8,128)(2,1)} %refs_0_.1, bf16[192,768]{1,0:T(8,128)(2,1)} %refs_1_.1, bf16[192,768]{1,0:T(8,128)(2,1)} %refs_2_.1, ...), custom_call_target="tpu_custom_call" | custom-call | tf_op jit(solution)/shard_map/pallas_call | solution.py:841
  113.5 2.2 %shard_map.128 = bf16[128,3072]{1,0:T(8,128)(2,1)} custom-call(bf16[128,3072]{1,0:T(8,128)(2,1)} %get-tuple-element.7.a_ref, bf16[128,3072]{1,0:T(8,128)(2,1)} %get-tuple-element.8.b_ref), custom_call_target="tpu_custom_call" | custom-call | tf_op jit(solution)/shard_map/pallas_call | solution.py:887

commit v6 on v5

--- a/solution.py
+++ b/solution.py
@@ -560,7 +560,7 @@
     outs.send_y(1, 0, inside)
     ins.on_z(3, 1, 1)
     add_both(1)
-    outs.send_y(1, 0, at_end)
+    outs.send_y(1, 0, at_end & (core == 0))
     outs.on_z(1, 1, 0, FAR, PAIR, inside)
     outs.on_z(2, 0, 0, FAR, only=inside)
 
@@ -611,6 +611,7 @@
             tails(1, 0, at.after, action)
 
     all_tails("start")
+    outs.send_y(1, 0, at_end & (core == 1))
     for r in range(2):
         outs.on_z(1, r, 0, FAR, PAIR, at_end)
     add_last(True)
@@ -775,13 +776,13 @@
     fold(2)
     fold(3)
     outs.on_z(1, 1, 0, NEAR, APART)
-    relay(0)
     outs.on_z(2, 1, 0, NEAR, only=inside)
     begin(4)
-    relay(1)
     begin(5)
     fold(4)
+    relay(0)
     fold(5)
+    relay(1)
     collect(0)
     collect(1)
     relay(2)

time: 116 us -> 117 us (level)
  no operation moved by 1% of the time
where the time goes in v6:
time: 117 us; the launch traced here: 116 us
  Pallas kernels  116 us (99%)
    pallas_call x1, Pallas kernels, whole_layer(): pl.pallas_call(functools.partial(layer_entry, count, chans, wide, split),...  114 us

profile of v6, /device:TPU:0, one launch (start us, length us, event | category | flops | bytes accessed | tf_op | source)
XLA Modules:
  0.0 115.8 jit_solution(18004128882732266321)
XLA Ops:
  0.0 113.5 %shard_map.127 = (bf16[128,3072]{1,0:T(8,128)(2,1)}, bf16[128,3072]{1,0:T(8,128)(2,1)}) custom-call(f32[24]{0:T(128)} %constant.2.clone.slopes_ref, f32[12]{0:T(128)} %sinks_ref.1, bf16[256,1536]{1,0:T(8,128)(2,1)} %tok_hbm.1, bf16[192,768]{1,0:T(8,128)(2,1)} %refs_0_.1, bf16[192,768]{1,0:T(8,128)(2,1)} %refs_1_.1, bf16[192,768]{1,0:T(8,128)(2,1)} %refs_2_.1, ...), custom_call_target="tpu_custom_call" | custom-call | tf_op jit(solution)/shard_map/pallas_call | solution.py:842
  113.6 2.2 %shard_map.128 = bf16[128,3072]{1,0:T(8,128)(2,1)} custom-call(bf16[128,3072]{1,0:T(8,128)(2,1)} %get-tuple-element.7.a_ref, bf16[128,3072]{1,0:T(8,128)(2,1)} %get-tuple-element.8.b_ref), custom_call_target="tpu_custom_call" | custom-call | tf_op jit(solution)/shard_map/pallas_call | solution.py:888

commit v7 on v5

--- a/solution.py
+++ b/solution.py
@@ -159,12 +159,12 @@
     def column(self, r):
         return self.at.x if r == 0 else 1 - self.at.x
 
-    def z_copy(self, up, d, r, t, s, send_d):
+    def z_copy(self, up, d, r, t, s):
         at = self.at
         dst = self.slot(t, self.origin(up, d), at.y, self.column(r), s)
         src = self.src.at[2 * t + at.x, self.part(s)] if d == 0 and r == 0 else dst
         side = 0 if up else 1
-        i = (((side * (at.layers - 1) + send_d) * 2 + r) * 2 + t) * self.split + s
+        i = ((self.origin(up, d) * 2 + r) * 2 + t) * self.split + s
         return remote(src, dst, self.zs.at[2 * side + t], self.zr.at[i], at.above if up else at.below)
 
     def z_send(self, up, d, r, t, s, only=True):
@@ -178,13 +178,13 @@
 
         @pl.when(go & only)
         def _():
-            self.z_copy(up, d, r, t, s, d).start()
+            self.z_copy(up, d, r, t, s).start()
 
     def y_copy(self, up, d, r, s, y):
         at = self.at
         dst = self.slot(at.zl, self.origin(up, d), y, self.column(r), s)
         src = self.src.at[2 * at.zl + at.x, self.part(s)] if d == 0 and r == 0 else dst
-        m = d if up or d == 0 else at.layers - 1 + d
+        m = self.origin(up, d)
         return remote(src, dst, self.ys.at[0], self.yr.at[m], at.ypeer)
 
     def x_copy(self, t, s, receive=False):
@@ -227,7 +227,7 @@
 
             @pl.when(here & only)
             def _():
-                self.z_copy(up, d, r, t, s, d - 1).wait_recv()
+                self.z_copy(up, d, r, t, s).wait_recv()
                 self.z_send(up, d, r, t, s)
 
                 @pl.when(zl == t)
@@ -243,7 +243,7 @@
 
         def each(up):
             ref = self.buf.at[zl, self.origin(up, d), 1 - y]
-            m = d if up or d == 0 else layers - 1 + d
+            m = self.origin(up, d)
             remote(ref, ref, self.ys.at[0], self.yr.at[m], self.at.ypeer).wait_recv()
 
         if d == 0 or up is not None:
@@ -834,8 +834,8 @@
     chunks = 2 * layers
 
     def sems(parts):
-        hops = 2 * (layers - 1) * 4 * parts
-        return [dma((number,)) for number in (4, hops, 1, 2 * layers - 1, 1, 2 * parts)]
+        hops = layers * 4 * parts
+        return [dma((number,)) for number in (4, hops, 1, layers, 1, 2 * parts)]
 
     smem = pl.BlockSpec(memory_space=pltpu.SMEM)
     return pl.pallas_call(

time: 116 us -> 116 us (level)
  no operation moved by 1% of the time
where the time goes in v7:
time: 116 us
  Pallas kernels  116 us (100%)
    pallas_call x1, Pallas kernels, whole_layer(): pl.pallas_call(functools.partial(layer_entry, count, chans, wide, split),...  113 us

profile of v7, /device:TPU:0, one launch (start us, length us, event | category | flops | bytes accessed | tf_op | source)
XLA Modules:
  0.0 115.5 jit_solution(1399900874582574772)
XLA Ops:
  0.0 113.3 %shard_map.127 = (bf16[128,3072]{1,0:T(8,128)(2,1)}, bf16[128,3072]{1,0:T(8,128)(2,1)}) custom-call(f32[24]{0:T(128)} %constant.2.clone.slopes_ref, f32[12]{0:T(128)} %sinks_ref.1, bf16[256,1536]{1,0:T(8,128)(2,1)} %tok_hbm.1, bf16[192,768]{1,0:T(8,128)(2,1)} %refs_0_.1, bf16[192,768]{1,0:T(8,128)(2,1)} %refs_1_.1, bf16[192,768]{1,0:T(8,128)(2,1)} %refs_2_.1, ...), custom_call_target="tpu_custom_call" | custom-call | tf_op jit(solution)/shard_map/pallas_call | solution.py:841
  113.3 2.2 %shard_map.128 = bf16[128,3072]{1,0:T(8,128)(2,1)} custom-call(bf16[128,3072]{1,0:T(8,128)(2,1)} %get-tuple-element.7.a_ref, bf16[128,3072]{1,0:T(8,128)(2,1)} %get-tuple-element.8.b_ref), custom_call_target="tpu_custom_call" | custom-call | tf_op jit(solution)/shard_map/pallas_call | solution.py:887
